TPU v7x, 32 devices: a whole 2x2x4 slice. The times are simulated.
32 devices in a mesh: sp: 4 (over y, x), tp: 8 (over z, core).
Axes of the slice: x: 2, y: 2, z: 4, core: 2. Of those that a mesh axis runs over, the one named last changes fastest.
Arguments:
- moe_input: bfloat16 [512, 2048], P('sp'), may hold values from -6 to 6
- cotangent: bfloat16 [512, 2048], P('sp'), may hold values from -6 to 6
- route_expert: int32 [512, 2], P('sp'), may hold values from 0 to 3, all different within a row; in each aligned block of 128 rows (0 to 127, 128 to 255, ...) at most 128 rows name the same one
- route_weight: float32 [512, 2], P('sp'), may hold values from 0.2 to 1
- w_gate: bfloat16 [4, 2048, 6144], P('sp', None, 'tp'), may hold values from -0.125 to 0.125
- w_up: bfloat16 [4, 2048, 6144], P('sp', None, 'tp'), may hold values from -0.125 to 0.125
- w_down: bfloat16 [4, 6144, 2048], P('sp', 'tp'), may hold values from -0.078125 to 0.078125
- out_proj: bfloat16 [2048, 2048], P('tp'), may hold values from -0.125 to 0.125
- saved_out: bfloat16 [512, 2048], P('sp', 'tp'), may hold values from -6 to 6
- queries: bfloat16 [512, 1024], P('sp', 'tp'), may hold values from -6 to 6
- keys: bfloat16 [512, 1024], P('sp', 'tp'), may hold values from -6 to 6
- values: bfloat16 [512, 2048], P('sp', 'tp'), may hold values from -6 to 6
- log_decay: float32 [512, 1024], P('sp', 'tp'), may hold values from -1 to 0
- span_state: float32 [8, 1024, 128], P('sp', 'tp'), may hold values from -6 to 6
Outputs:
- grad_w_gate: bfloat16 [4, 2048, 6144], P('sp', None, 'tp')
- grad_w_up: bfloat16 [4, 2048, 6144], P('sp', None, 'tp')
- grad_w_down: bfloat16 [4, 6144, 2048], P('sp', 'tp')
- grad_proj: float32 [2048, 2048], P('sp', 'tp')
- grad_queries: bfloat16 [512, 1024], P('sp', 'tp')
- grad_keys: bfloat16 [512, 1024], P('sp', 'tp')
- grad_values: bfloat16 [512, 2048], P('sp', 'tp')
- grad_decay: float32 [512, 1024], P('sp', 'tp')
Inputs may be any that keep to these rules, and one draw needn't show every extreme that they name: `route_expert`: each row names two different experts. Within the 128 rows of one index of sp no expert is named by more than 128 rows, a bound that some block reaches.
All inputs are finite; a program needn't handle non-finite values.
Results may differ from a plain program's by a relative error of at most 0.019.
Values may be sent and summed in bfloat16 or wider, within the bound.
No kernel may reach another device: no remote copies, remote signals or barrier semaphores. Data moves between devices by JAX's collectives and lax.ppermute only.
A program may use at most 128 MiB of HBM per device.

v0:
```python
import jax
import jax.numpy as jnp
from jax import lax
from jax.sharding import PartitionSpec as P

DK = 64
SPAN = 64


HIGH = lax.Precision.HIGHEST


def entering(shard, axis, combine, identity):
    length, mine = (lax.axis_size(axis), lax.axis_index(axis))
    everything = jax.tree.map(lambda part: lax.all_gather(part, axis), shard)
    start = jax.tree.map(
        lambda part, zero: jnp.broadcast_to(jnp.asarray(zero, part.dtype), part.shape),
        shard,
        identity,
    )

    def step(k, before):
        at = length - 1 - k
        reached = at > mine
        new = combine(before, jax.tree.map(lambda part: part[at], everything))
        return jax.tree.map(lambda a, b: jnp.where(reached, a, b), new, before)

    return lax.fori_loop(0, length, step, start)


def slot_places(experts, count):
    routes_flat = experts.reshape(-1)
    one_hot = (routes_flat[:, None] == jnp.arange(count, dtype=jnp.int32)[None, :]).astype(
        jnp.int32
    )
    earlier = jnp.cumsum(one_hot, axis=0) - one_hot
    return jnp.sum(earlier * one_hot, axis=1).reshape(experts.shape)


def expert_grads(inputs, routed, gate_weight, up_weight, down_weight):
    gate = jnp.dot(inputs, gate_weight, preferred_element_type=jnp.float32)
    upper = jnp.dot(inputs, up_weight, preferred_element_type=jnp.float32)
    sigmoid_gate = jax.nn.sigmoid(gate)
    active = gate * sigmoid_gate
    hidden = (active * upper).astype(jnp.bfloat16)
    d_hidden = lax.dot_general(
        routed, down_weight, (((1,), (1,)), ((), ())), preferred_element_type=jnp.float32
    )
    d_upper = (d_hidden * active).astype(jnp.bfloat16)
    d_gate = (d_hidden * upper * sigmoid_gate * (1.0 + gate * (1.0 - sigmoid_gate))).astype(
        jnp.bfloat16
    )
    grad_down = lax.dot_general(
        hidden, routed, (((0,), (0,)), ((), ())), preferred_element_type=jnp.float32
    ).astype(jnp.bfloat16)
    grad_gate = lax.dot_general(
        inputs, d_gate, (((0,), (0,)), ((), ())), preferred_element_type=jnp.float32
    ).astype(jnp.bfloat16)
    grad_up = lax.dot_general(
        inputs, d_upper, (((0,), (0,)), ((), ())), preferred_element_type=jnp.float32
    ).astype(jnp.bfloat16)
    return (d_gate, d_upper, grad_gate, grad_up, grad_down)


def input_grad(d_gate, d_upper, gate_weight, up_weight):
    first = lax.dot_general(
        d_gate, gate_weight, (((1,), (1,)), ((), ())), preferred_element_type=jnp.float32
    )
    second = lax.dot_general(
        d_upper, up_weight, (((1,), (1,)), ((), ())), preferred_element_type=jnp.float32
    )
    return first + second


def gated_pieces(queries, keys, values, log_decay, grad_mix, key_dim, span_len):
    value_dim = values.shape[1] * key_dim // queries.shape[1]
    heads = queries.shape[1] // key_dim
    spans = queries.shape[0] // span_len

    def blocks(array, width):
        return array.astype(jnp.float32).reshape(spans, span_len, heads, width)

    query_spans = blocks(queries, key_dim)
    key_spans = blocks(keys, key_dim)
    value_spans = blocks(values, value_dim)
    grad_spans = blocks(grad_mix, value_dim)
    cumulative = jnp.cumsum(blocks(log_decay, key_dim), axis=1)
    last = cumulative[:, -1]
    scale = key_dim ** (-0.5)
    query_decayed = query_spans * jnp.exp(cumulative)
    key_grown = key_spans * jnp.exp(-cumulative)
    key_to_end = key_spans * jnp.exp(last[:, None] - cumulative)
    g_local = scale * jnp.einsum("nthk,nthv->nhkv", query_decayed, grad_spans, precision=HIGH)
    return (
        query_spans,
        key_spans,
        value_spans,
        grad_spans,
        cumulative,
        last,
        query_decayed,
        key_grown,
        key_to_end,
        g_local,
    )


def backward_step(carry, inputs):
    local, decay = inputs
    return (local + jnp.exp(decay)[..., None] * carry, carry)


def gated_finish(pieces, span_state, g_end, key_dim):
    (
        query_spans,
        key_spans,
        value_spans,
        grad_spans,
        cumulative,
        last,
        query_decayed,
        key_grown,
        key_to_end,
        g_local,
    ) = pieces
    spans, span_len, heads, value_dim = value_spans.shape
    scale = key_dim ** (-0.5)
    token_locations = jnp.arange(span_len, dtype=jnp.int32)
    causal = (token_locations[:, None] >= token_locations[None, :]).astype(jnp.float32)
    scores = jnp.einsum("nthk,nshk->nhts", query_decayed, key_grown, precision=HIGH) * causal
    grad_dot = jnp.einsum("nthv,nshv->nhts", grad_spans, value_spans, precision=HIGH) * causal
    state = span_state.reshape(spans, heads, key_dim, value_dim)
    d_query = (
        scale
        * jnp.exp(cumulative)
        * (
            jnp.einsum("nhts,nshk->nthk", grad_dot, key_grown, precision=HIGH)
            + jnp.einsum("nthv,nhkv->nthk", grad_spans, state, precision=HIGH)
        )
    )
    d_key = scale * jnp.exp(-cumulative) * jnp.einsum(
        "nhts,nthk->nshk", grad_dot, query_decayed, precision=HIGH
    ) + jnp.exp(last[:, None] - cumulative) * jnp.einsum(
        "nshv,nhkv->nshk", value_spans, g_end, precision=HIGH
    )
    d_value = scale * jnp.einsum(
        "nhts,nthv->nshv", scores, grad_spans, precision=HIGH
    ) + jnp.einsum("nshk,nhkv->nshv", key_to_end, g_end, precision=HIGH)
    state_end = jnp.exp(last)[..., None] * state + jnp.einsum(
        "nshk,nshv->nhkv", key_to_end, value_spans, precision=HIGH
    )
    tail = jnp.sum(state_end * g_end, axis=-1)
    d_cumulative = query_spans * d_query - key_spans * d_key
    d_log = jnp.cumsum(d_cumulative[:, ::-1], axis=1)[:, ::-1] + tail[:, None]
    rows = spans * span_len
    return (
        d_query.reshape(rows, heads * key_dim).astype(jnp.bfloat16),
        d_key.reshape(rows, heads * key_dim).astype(jnp.bfloat16),
        d_value.reshape(rows, heads * value_dim).astype(jnp.bfloat16),
        d_log.reshape(rows, heads * key_dim),
    )


def carry_combine(earlier, later):
    return (later[0] * earlier[0], later[1] + later[0][..., None] * earlier[1])


def on_device(
    moe_input,
    cotangent,
    route_expert,
    route_weight,
    w_gate,
    w_up,
    w_down,
    out_proj,
    saved_out,
    queries,
    keys,
    values,
    log_decay,
    span_state,
):
    tok_rows, width = moe_input.shape
    groups = lax.axis_size("sp")
    lanes = lax.axis_size("tp")
    capacity = 4 * tok_rows // groups
    target_locations = slot_places(route_expert, groups)
    rows_index = (target_locations * groups + route_expert).reshape(-1)
    owner = (
        jnp.full((capacity * groups,), 2 * tok_rows, jnp.int32)
        .at[rows_index]
        .set(jnp.arange(2 * tok_rows, dtype=jnp.int32))
    )
    weighted = (route_weight[:, :, None] * cotangent[:, None, :].astype(jnp.float32)).astype(
        jnp.bfloat16
    )
    weighted = weighted.reshape(2 * tok_rows, width)
    blank = jnp.zeros((1, width), jnp.bfloat16)
    send_in = jnp.concatenate([moe_input, blank], axis=0)[owner // 2].reshape(
        capacity, groups, width
    )
    send_cot = jnp.concatenate([weighted, blank], axis=0)[owner].reshape(capacity, groups, width)
    gate_weight = w_gate[0]
    up_weight = w_up[0]
    down_weight = w_down[0]
    share = capacity // lanes
    lane = lax.axis_index("tp")
    part_in = lax.dynamic_slice_in_dim(send_in, lane * share, share, 0)
    part_cot = lax.dynamic_slice_in_dim(send_cot, lane * share, share, 0)
    got_in, got_cot = (
        lax.all_to_all(part_in, "sp", split_axis=1, concat_axis=1, tiled=True),
        lax.all_to_all(part_cot, "sp", split_axis=1, concat_axis=1, tiled=True),
    )
    full_in, full_cot = (
        lax.all_gather(got_in, "tp", axis=0, tiled=True),
        lax.all_gather(got_cot, "tp", axis=0, tiled=True),
    )
    d_gate, d_upper, grad_gate, grad_up, grad_down = expert_grads(
        full_in.reshape(-1, width), full_cot.reshape(-1, width), gate_weight, up_weight, down_weight
    )
    mine = (
        lax.psum_scatter(
            input_grad(d_gate, d_upper, gate_weight, up_weight).astype(jnp.bfloat16),
            "tp",
            scatter_dimension=0,
            tiled=True,
        )
        .astype(jnp.float32)
        .reshape(share, groups, width)
    )
    returned = (
        lax.all_to_all(mine.astype(jnp.bfloat16), "sp", split_axis=1, concat_axis=1, tiled=True)
        .astype(mine.dtype)
        .reshape(-1, width)
    )
    local_index = rows_index - lane * share * groups
    inside = (local_index >= 0) & (local_index < share * groups)
    picked = jnp.where(inside[:, None], returned[jnp.clip(local_index, 0, share * groups - 1)], 0.0)
    routed = jnp.sum(picked.reshape(tok_rows, 2, width), axis=1)
    total = lax.psum(routed.astype(jnp.bfloat16), "tp").astype(jnp.float32)
    grad_in = (cotangent.astype(jnp.float32) + total).astype(jnp.bfloat16)
    grad_mix = lax.dot_general(
        grad_in, out_proj, (((1,), (1,)), ((), ())), preferred_element_type=jnp.float32
    )
    grad_proj = lax.psum_scatter(
        lax.dot_general(
            grad_in, saved_out, (((0,), (0,)), ((), ())), preferred_element_type=jnp.float32
        ).astype(jnp.bfloat16),
        "sp",
        scatter_dimension=0,
        tiled=True,
    ).astype(jnp.float32)
    pieces = gated_pieces(queries, keys, values, log_decay, grad_mix, DK, SPAN)
    g_local = pieces[9]
    last = pieces[5]
    begin = jnp.zeros(g_local.shape[1:], jnp.float32)
    device_start, local_end = lax.scan(backward_step, begin, (g_local, last), reverse=True)
    device_decay = jnp.exp(jnp.sum(last, axis=0))
    identity = (jnp.ones_like(device_decay), jnp.zeros_like(device_start))
    decay_after, state_after = entering((device_decay, device_start), "sp", carry_combine, identity)
    running = jnp.cumsum(last, axis=0)
    beyond = running[-1][None] - running
    g_end = local_end + jnp.exp(beyond)[..., None] * state_after[None]
    grad_queries, grad_keys, grad_values, grad_decay = gated_finish(pieces, span_state, g_end, DK)
    return (
        grad_gate[None],
        grad_up[None],
        grad_down[None],
        grad_proj,
        grad_queries,
        grad_keys,
        grad_values,
        grad_decay,
    )


def solution(mesh):
    placed = (
        P("sp", None),
        P("sp", None),
        P("sp", None),
        P("sp", None),
        P("sp", None, "tp"),
        P("sp", None, "tp"),
        P("sp", "tp", None),
        P("tp", None),
        P("sp", "tp"),
        P("sp", "tp"),
        P("sp", "tp"),
        P("sp", "tp"),
        P("sp", "tp"),
        P("sp", "tp", None),
    )
    return jax.shard_map(
        on_device,
        mesh=mesh,
        in_specs=placed,
        out_specs=(
            P("sp", None, "tp"),
            P("sp", None, "tp"),
            P("sp", "tp", None),
            P("sp", "tp"),
            P("sp", "tp"),
            P("sp", "tp"),
            P("sp", "tp"),
            P("sp", "tp"),
        ),
        check_vma=False,
    )
```

profile of v0, /device:TPU:0, one launch (start us, length us, event | category | flops | bytes accessed | tf_op | source)
XLA Modules:
  0.0 273.4 jit_solution(1842844893253880070)
XLA Ops:
  14.6 6.3 %gather_fusion = bf16[512,2048]{1,0:T(8,128)(2,1)} fusion(bf16[129,2048]{1,0:T(8,128)(2,1)} %concatenate.6, s32[1024]{0:T(1024)S(1)} %get-tuple-element.318), kind=kCustom, calls=%fused_computation | custom fusion | bytes 4196352 | tf_op jit(solution)/shard_map/gather | solution.py:200
  21.0 4.1 %reshape.208 = bf16[128,4,2048]{2,1,0:T(4,128)(2,1)} reshape(bf16[512,2048]{1,0:T(8,128)(2,1)} %gather_fusion) | data formatting | bytes 4194304 | tf_op jit(solution)/shard_map/reshape | solution.py:200
  26.3 10.7 %all_to_all.15 = bf16[16,4,2048]{2,0,1:T(8,128)(2,1)S(1)} all-to-all(bf16[16,4,2048]{2,0,1:T(8,128)(2,1)S(1)} %copy.146), channel_id=1, replica_groups=mesh['sp'=4,'tp'=8] {'sp'}, dimensions={1} | all-to-all | bytes 524288 | tf_op jit(solution)/shard_map/all_to_all | solution.py:212
  38.0 3.4 %mul.203 = f32[128,2,2048]{2,1,0:T(2,128)} broadcast(bf16[128,2048]{1,0:T(8,128)(2,1)} %param.19), dimensions={0,2} | broadcast | bytes 2621440 | tf_op jit(solution)/shard_map/mul | solution.py:195
  41.4 3.7 %mul.204 = f32[256,2048]{1,0:T(8,128)} reshape(f32[128,2,2048]{2,1,0:T(2,128)} %mul.203) | data formatting | bytes 4194304 | tf_op jit(solution)/shard_map/mul | solution.py:195
  48.3 6.6 %gather_fusion.1 = bf16[512,2048]{1,0:T(8,128)(2,1)} fusion(bf16[257,2048]{1,0:T(8,128)(2,1)} %concatenate.7, s32[1024]{0:T(1024)S(1)} %get-tuple-element.317), kind=kCustom, calls=%fused_computation.1 | custom fusion | bytes 4196352 | tf_op jit(solution)/shard_map/gather | solution.py:203
  54.9 4.1 %reshape.210 = bf16[128,4,2048]{2,1,0:T(4,128)(2,1)} reshape(bf16[512,2048]{1,0:T(8,128)(2,1)} %gather_fusion.1) | data formatting | bytes 4194304 | tf_op jit(solution)/shard_map/reshape | solution.py:203
  60.2 8.1 %all_to_all.16 = bf16[16,4,2048]{2,0,1:T(8,128)(2,1)S(1)} all-to-all(bf16[16,4,2048]{2,0,1:T(8,128)(2,1)S(1)} %copy.147), channel_id=1, replica_groups=mesh['sp'=4,'tp'=8] {'sp'}, dimensions={1} | all-to-all | bytes 524288 | tf_op jit(solution)/shard_map/all_to_all | solution.py:213
  69.5 3.9 %reshape.209 = bf16[512,2048]{1,0:T(8,128)(2,1)} reshape(bf16[128,4,2048]{2,1,0:T(4,128)(2,1)} %all-gather.6.cloned.1.call-done) | data formatting | bytes 4194304 | tf_op jit(solution)/shard_map/reshape | solution.py:220
  73.5 4.7 %fusion.3 = f32[512,768]{1,0:T(8,128)} fusion(bf16[512,2048]{1,0:T(8,128)(2,1)} %reshape.209, bf16[1,2048,768]{2,1,0:T(8,128)(2,1)S(1)} %copy-done), kind=kOutput, calls=%fused_computation.16 | convolution fusion | flops 1610612736 | bytes 6815744 | tf_op jit(solution)/shard_map/dot_general | solution.py:41
  81.1 17.2 %all-gather.8.cloned.1.call-done = bf16[128,4,2048]{2,1,0:T(4,128)(2,1)} async-done(((bf16[16,4,2048]{2,1,0:T(4,128)(2,1)}), bf16[128,4,2048]{2,1,0:T(4,128)(2,1)}) %all-gather.8.cloned.1.call-update) | async-done | bytes 2097168 | tf_op jit(solution)/shard_map/all_gather | solution.py:217
  98.3 3.9 %reshape.211 = bf16[512,2048]{1,0:T(8,128)(2,1)} reshape(bf16[128,4,2048]{2,1,0:T(4,128)(2,1)} %all-gather.8.cloned.1.call-done) | data formatting | bytes 4194304 | tf_op jit(solution)/shard_map/reshape | solution.py:220
  102.3 5.6 %multiply_convert_fusion.2 = (bf16[512,768]{1,0:T(8,128)(2,1)S(1)}, bf16[512,768]{1,0:T(8,128)(2,1)S(1)}) fusion(f32[512,768]{1,0:T(8,128)} %fusion.3, f32[512,768]{1,0:T(8,128)} %fusion.7, bf16[512,2048]{1,0:T(8,128)(2,1)} %reshape.211, bf16[1,768,2048]{2,1,0:T(8,128)(2,1)} %param.24), kind=kOutput, calls=%fused_computation.31 | convolution fusion | flops 1615724544 | bytes 9961472 | tf_op jit(solution)/shard_map/dot_general | solution.py:46
  110.4 3.2 %add_convert_fusion = bf16[512,2048]{1,0:T(8,128)(2,1)} fusion(f32[512,2048]{1,0:T(8,128)S(1)} %fusion.1, bf16[512,768]{1,0:T(8,128)(2,1)S(1)} %get-tuple-element.305, bf16[1,2048,768]{2,1,0:T(8,128)(2,1)S(1)} %copy-done.18), kind=kOutput, calls=%fused_computation.10 | convolution fusion | flops 1612709888 | bytes 10223616 | tf_op jit(solution)/shard_map/dot_general | solution.py:69
  115.3 8.0 %all-gather.2 = f32[4,2,64]{2,1,0:T(2,128)S(1)} all-gather(f32[1,2,64]{2,1,0:T(2,128)S(1)} %exponential_bitcast_fusion.1), channel_id=3, replica_groups=mesh['sp'=4,'tp'=8] {'sp'}, dimensions={0}, use_global_device_ids=true | all-gather | bytes 2560 | tf_op jit(solution)/shard_map/all_gather | solution.py:15
  124.4 6.3 %fusion.13 = bf16[1,768,2048]{2,1,0:T(8,128)(2,1)} fusion(bf16[512,2048]{1,0:T(8,128)(2,1)} %reshape.211, f32[512,768]{1,0:T(8,128)} %fusion.7, f32[512,768]{1,0:T(8,128)} %fusion.3), kind=kOutput, calls=%fused_computation.26 | convolution fusion | flops 1614544896 | bytes 8388608 | tf_op jit(solution)/shard_map/dot_general | solution.py:53
  130.7 18.3 %reduce-scatter.3.cloned.1.call-done = bf16[64,2048]{1,0:T(8,128)(2,1)} async-done(((bf16[512,2048]{1,0:T(8,128)(2,1)}), bf16[64,2048]{1,0:T(8,128)(2,1)}) %reduce-scatter.3.cloned.1.call-update) | async-done | bytes 262160 | tf_op jit(solution)/shard_map/reduce_scatter | solution.py:223
  150.9 3.8 %all-to-all-start.2 = ((bf16[16,4,2048]{2,0,1:T(8,128)(2,1)}), bf16[16,4,2048]{2,0,1:T(8,128)(2,1)S(1)}, u32[]{:S(2)}, u32[]{:S(2)}) async-start(bf16[16,4,2048]{2,0,1:T(8,128)(2,1)} %copy.115), calls=%async_computation.3 | async-start | bytes 524288 | tf_op jit(solution)/shard_map/all_to_all | solution.py:233
  154.7 4.6 %fusion.12 = bf16[1,2048,768]{2,1,0:T(8,128)(2,1)} fusion(bf16[512,2048]{1,0:T(8,128)(2,1)S(1)} %copy-done.5, bf16[512,768]{1,0:T(8,128)(2,1)} %copy-done.19), kind=kOutput, calls=%fused_computation.25 | convolution fusion | flops 1612185600 | bytes 6029312 | tf_op jit(solution)/shard_map/dot_general | solution.py:59
  164.2 5.8 %select_reduce_fusion = bf16[128,2048]{1,0:T(8,128)(2,1)} fusion(f32[128,2,2048]{2,1,0:T(2,128)} %gather.14, pred[128,2]{1,0:T(8,128)(4,1)S(1)} %copy.114), kind=kLoop, calls=%fused_computation.28 | loop fusion | flops 786432 | bytes 2621696 | tf_op jit(solution)/shard_map/reduce_sum | solution.py:240
  170.2 4.7 %fusion.11 = bf16[1,2048,768]{2,1,0:T(8,128)(2,1)} fusion(bf16[512,2048]{1,0:T(8,128)(2,1)S(1)} %copy-done.6, bf16[512,768]{1,0:T(8,128)(2,1)} %copy-done.20), kind=kOutput, calls=%fused_computation.24 | convolution fusion | flops 1612185600 | bytes 6029312 | tf_op jit(solution)/shard_map/dot_general | solution.py:56
  174.9 49.9 %all-reduce.4.cloned.1.call-done = bf16[128,2048]{1,0:T(8,128)(2,1)} async-done(((bf16[128,2048]{1,0:T(8,128)(2,1)}), bf16[128,2048]{1,0:T(8,128)(2,1)}) %all-reduce.4.cloned.1.call-update) | async-done | bytes 524304 | tf_op jit(solution)/shard_map/psum | solution.py:241
  227.4 9.5 %all-gather = f32[8,64,128]{2,1,0:T(8,128)S(1)} all-gather(f32[2,64,128]{2,1,0:T(8,128)S(1)} %get-tuple-element.245), channel_id=2, replica_groups=mesh['sp'=4,'tp'=8] {'sp'}, dimensions={0}, use_global_device_ids=true | all-gather | bytes 327680 | tf_op jit(solution)/shard_map/all_gather | solution.py:15
  255.4 9.7 %reduce-scatter.5.cloned.1.call-done = bf16[512,256]{1,0:T(8,128)(2,1)} async-done(((bf16[2048,256]{1,0:T(8,128)(2,1)}), bf16[512,256]{1,0:T(8,128)(2,1)}) %reduce-scatter.5.cloned.1.call-update) | async-done | bytes 262160 | tf_op jit(solution)/shard_map/reduce_scatter | solution.py:246
  (157 shorter events, 53.4 us)
Async XLA Ops:
  7.2 66.3 %copy-start = (bf16[1,2048,768]{2,1,0:T(8,128)(2,1)S(1)}, bf16[1,2048,768]{2,1,0:T(8,128)(2,1)}, u32[]{:S(2)}) copy-start(bf16[1,2048,768]{2,1,0:T(8,128)(2,1)} %param.22) | copy-start | bytes 9437188
  7.2 62.3 %all-gather.6.cloned.1.call-start = ((), (), s32[]{:S(2)}) async-start(), calls=%async_computation.5 | async-start | bytes 2359296 | tf_op jit(solution)/shard_map/all_gather | solution.py:216
  38.0 60.4 %all-gather.8.cloned.1.call-start = ((), (), s32[]{:S(2)}) async-start(), calls=%async_computation.6 | async-start | bytes 2359296 | tf_op jit(solution)/shard_map/all_gather | solution.py:217
  41.4 3.7 %copy-start.16 = (f32[128,2]{0,1:T(2,128)S(1)}, f32[128,2]{0,1:T(2,128)}, u32[]{:S(2)}) copy-start(f32[128,2]{0,1:T(2,128)} %param.21) | copy-start | bytes 3076
  69.3 79.7 %reduce-scatter.3.cloned.1.call-start = ((), (), s32[]{:S(2)}) async-start(), calls=%async_computation.7 | async-start | bytes 2359296 | tf_op jit(solution)/shard_map/reduce_scatter | solution.py:223
  73.5 4.7 %copy-start.4 = (bf16[512,2048]{1,0:T(8,128)(2,1)S(1)}, bf16[512,2048]{1,0:T(8,128)(2,1)}, u32[]{:S(2)}) copy-start(bf16[512,2048]{1,0:T(8,128)(2,1)} %reshape.209) | copy-start | bytes 6291460
  73.5 4.7 %copy-start.17 = (bf16[1,2048,768]{2,1,0:T(8,128)(2,1)S(1)}, bf16[1,2048,768]{2,1,0:T(8,128)(2,1)}, u32[]{:S(2)}) copy-start(bf16[1,2048,768]{2,1,0:T(8,128)(2,1)} %param.23) | copy-start | bytes 9437188
  107.9 1.9 copy-start.20
  107.9 1.9 copy-start.19
  107.9 2.5 copy-start.18
  113.6 1.7 copy-start.13
  124.4 30.3 %copy-start.5 = (bf16[512,2048]{1,0:T(8,128)(2,1)S(1)}, bf16[512,2048]{1,0:T(8,128)(2,1)}, u32[]{:S(2)}) copy-start(bf16[512,2048]{1,0:T(8,128)(2,1)} %reshape.209) | copy-start | bytes 6291460
  150.9 9.2 %all-to-all-start.2 = ((bf16[16,4,2048]{2,0,1:T(8,128)(2,1)}), bf16[16,4,2048]{2,0,1:T(8,128)(2,1)S(1)}, u32[]{:S(2)}, u32[]{:S(2)}) async-start(bf16[16,4,2048]{2,0,1:T(8,128)(2,1)} %copy.115), calls=%async_computation.3 | async-start | bytes 524288 | tf_op jit(solution)/shard_map/all_to_all | solution.py:233
  154.7 70.0 %all-reduce.4.cloned.1.call-start = ((), (), s32[]{:S(2)}) async-start(), calls=%async_computation.8 | async-start | bytes 1048576 | tf_op jit(solution)/shard_map/psum | solution.py:241
  164.2 5.9 %copy-start.6 = (bf16[512,2048]{1,0:T(8,128)(2,1)S(1)}, bf16[512,2048]{1,0:T(8,128)(2,1)}, u32[]{:S(2)}) copy-start(bf16[512,2048]{1,0:T(8,128)(2,1)} %reshape.209) | copy-start | bytes 6291460
  170.1 54.6 %copy-start.2 = (bf16[128,2048]{1,0:T(8,128)(2,1)S(1)}, bf16[128,2048]{1,0:T(8,128)(2,1)}, u32[]{:S(2)}) copy-start(bf16[128,2048]{1,0:T(8,128)(2,1)} %param.19) | copy-start | bytes 1572868
  170.1 95.0 %reduce-scatter.5.cloned.1.call-start = ((), (), s32[]{:S(2)}) async-start(), calls=%async_computation.9 | async-start | bytes 1310720 | tf_op jit(solution)/shard_map/reduce_scatter | solution.py:246
  226.6 10.8 %copy-start.7 = (bf16[128,2048]{1,0:T(8,128)(2,1)S(1)}, bf16[128,2048]{1,0:T(8,128)(2,1)}, u32[]{:S(2)}) copy-start(bf16[128,2048]{1,0:T(8,128)(2,1)} %all-reduce.4.cloned.1.call-done) | copy-start | bytes 1572868
  226.6 10.8 %copy-start.12 = (bf16[128,256]{1,0:T(8,128)(2,1)S(1)}, bf16[128,256]{1,0:T(8,128)(2,1)}, u32[]{:S(2)}) copy-start(bf16[128,256]{1,0:T(8,128)(2,1)} %param.26) | copy-start | bytes 196612
  226.7 12.5 %copy-start.3 = (f32[2,64,2,128]{3,2,1,0:T(2,128)}, f32[2,64,2,128]{3,2,1,0:T(2,128)S(1)}, u32[]{:S(2)}) copy-start(f32[2,64,2,128]{3,2,1,0:T(2,128)S(1)} %reshape.217) | copy-start | bytes 393220
  227.4 12.2 %copy-start.8 = (f32[2,2,64,128]{3,2,1,0:T(8,128)}, f32[2,2,64,128]{3,2,1,0:T(8,128)S(1)}, u32[]{:S(2)}) copy-start(f32[2,2,64,128]{3,2,1,0:T(8,128)S(1)} %get-tuple-element.244) | copy-start | bytes 393220
  237.5 1.7 copy-start.9
  241.2 25.7 %copy-start.1 = (bf16[1,2048,768]{2,1,0:T(8,128)(2,1)S(1)}, bf16[1,2048,768]{2,1,0:T(8,128)(2,1)}, u32[]{:S(2)}) copy-start(bf16[1,2048,768]{2,1,0:T(8,128)(2,1)} %param.22) | copy-start | bytes 9437188
  246.1 8.5 %copy-start.10 = (bf16[2,64,2,64]{1,3,2,0:T(8,128)(2,1)S(1)}, bf16[2,64,2,64]{1,3,2,0:T(8,128)(2,1)}, u32[]{:S(2)}) copy-start(bf16[2,64,2,64]{1,3,2,0:T(8,128)(2,1)} %get-tuple-element.309) | copy-start | bytes 98308
  (3 other events, 3.4 us)
Sparse Core Ops, SparseCore 0:
  38.1 28.8 all-gather.5
  69.4 28.8 all-gather.7
  113.7 35.2 reduce-scatter.2
  170.2 54.4 all-reduce.3
  239.1 26.0 reduce-scatter.4
where the time goes:
time: 275 us; the launch traced here: 273 us
  waiting for transfers between devices  95.9 us (35%)
  local copies, waits for them, and re-layouts  63.6 us (23%)
  matrix products  44.8 us (16%)
  blocking collectives  36.4 us (13%)
  between operations  14.4 us (5%)
  other arithmetic  14 us (5%)
  starting transfers between devices  4.16 us (2%)
    psum x1, waiting for transfers between devices, on_device(): total = lax.psum(routed.astype(jnp.bfloat16), 'tp').astype(jnp.float32)  49.9 us
    reduce_scatter x1, waiting for transfers between devices, on_device(): lax.psum_scatter(input_grad(d_gate, d_upper, gate_weight, up_weight).asty...  18.3 us
    all_gather x2, blocking collectives, entering(): everything = jax.tree.map(lambda part: lax.all_gather(part, axis), shard)  17.5 us
    all_gather x1, waiting for transfers between devices, on_device(): lax.all_gather(got_cot, 'tp', axis=0, tiled=True)  17.2 us
    all_to_all x1, blocking collectives, on_device(): lax.all_to_all(part_in, 'sp', split_axis=1, concat_axis=1, tiled=True)  10.7 us
    reduce_scatter x1, waiting for transfers between devices, on_device(): lax.psum_scatter(lax.dot_general(grad_in, saved_out, (((0,), (0,)), ((),...  9.71 us
    all_to_all x1, blocking collectives, on_device(): lax.all_to_all(part_cot, 'sp', split_axis=1, concat_axis=1, tiled=True)  8.11 us
    mul x3, local copies, waits for them, and re-layouts, on_device(): route_weight[:, :, None] * cotangent[:, None, :].astype(jnp.float32)  7.21 us
  transfers between devices with their start and end apart: 6, of which 5 were waited for; matrix products, arithmetic and copies ran while one was open for 25% of the time, Pallas kernels for 0%

commit v1 on v0

--- a/solution.py
+++ b/solution.py
@@ -1,13 +1,22 @@
+import functools
+
 import jax
 import jax.numpy as jnp
 from jax import lax
+from jax.experimental import pallas as pl
+from jax.experimental.pallas import tpu as pltpu
 from jax.sharding import PartitionSpec as P
+
 
 DK = 64
 SPAN = 64
-
-
 HIGH = lax.Precision.HIGHEST
+BF = jnp.bfloat16
+F32 = jnp.float32
+
+
+VM = pl.BlockSpec(memory_space=pltpu.VMEM)
+HB = pl.BlockSpec(memory_space=pltpu.HBM)
 
 
 def entering(shard, axis, combine, identity):
@@ -121,7 +130,7 @@
         query_decayed,
         key_grown,
         key_to_end,
-        g_local,
+        _,
     ) = pieces
     spans, span_len, heads, value_dim = value_spans.shape
     scale = key_dim ** (-0.5)
@@ -165,7 +174,7 @@
     return (later[0] * earlier[0], later[1] + later[0][..., None] * earlier[1])
 
 
-def on_device(
+def by_slots(
     moe_input,
     cotangent,
     route_expert,
@@ -258,7 +267,7 @@
     device_start, local_end = lax.scan(backward_step, begin, (g_local, last), reverse=True)
     device_decay = jnp.exp(jnp.sum(last, axis=0))
     identity = (jnp.ones_like(device_decay), jnp.zeros_like(device_start))
-    decay_after, state_after = entering((device_decay, device_start), "sp", carry_combine, identity)
+    _, state_after = entering((device_decay, device_start), "sp", carry_combine, identity)
     running = jnp.cumsum(last, axis=0)
     beyond = running[-1][None] - running
     g_end = local_end + jnp.exp(beyond)[..., None] * state_after[None]
@@ -275,36 +284,581 @@
     )
 
 
+def nt(a, b):
+    return lax.dot_general(a, b, (((1,), (1,)), ((), ())), preferred_element_type=F32)
+
+
+def nn(a, b):
+    return lax.dot_general(a, b, (((1,), (0,)), ((), ())), preferred_element_type=F32)
+
+
+def swap(value, axis, mask):
+    size = lax.axis_size(axis)
+    return lax.ppermute(value, axis, [(i, i ^ mask) for i in range(size)])
+
+
+def in_vmem(*values):
+    return [pltpu.with_memory_space_constraint(value, pltpu.VMEM) for value in values]
+
+
+def in_hbm(*values):
+    return [pltpu.with_memory_space_constraint(value, pltpu.HBM) for value in values]
+
+
+def spot():
+    lane = lax.axis_index("tp")
+    return lax.axis_index("sp"), lane % 2, lane // 2
+
+
+def grant(mib):
+    return pltpu.CompilerParams(vmem_limit_bytes=mib * 1024 * 1024)
+
+
+def packed_weights(expert_ref, weight_ref):
+    rows = expert_ref.shape[1]
+    line = lax.broadcasted_iota(jnp.int32, (rows, rows), 0)
+    table = jnp.zeros((rows, rows), F32)
+    for choice in range(expert_ref.shape[0]):
+        left = weight_ref[choice : choice + 1, :]
+        named = line % 8 == expert_ref[choice : choice + 1, :]
+        for part in range(3):
+            piece = left.astype(BF).astype(F32)
+            left = left - piece
+            table = table + jnp.where(named & (line // 8 == part), piece, 0.0)
+    return table.T
+
+
+def column_of(table, expert):
+    lane = lax.broadcasted_iota(jnp.int32, table.shape, 1)
+    picked = (lane % 8 == expert) & (lane < 24)
+    return jnp.sum(jnp.where(picked, table, 0.0), axis=1, keepdims=True)
+
+
+def prep_kernel(x_ref, cot_ref, expert_ref, weight_ref, first_ref, second_ref, e_ref, w_ref, table_ref, sems):
+    rows, width = x_ref.shape
+    _, core, _ = spot()
+    count = rows // 4
+    copies = [
+        pltpu.make_async_copy(expert_ref, e_ref, sems.at[0]),
+        pltpu.make_async_copy(weight_ref, w_ref, sems.at[1]),
+    ]
+    for at, out in enumerate((first_ref, second_ref)):
+        block = pl.ds(pl.multiple_of(core * 2 * count + at * count, count), count)
+        for side, source in enumerate((x_ref, cot_ref)):
+            target = out.at[:, pl.ds(side * width, width)]
+            copies.append(pltpu.make_async_copy(source.at[block, :], target, sems.at[2 + 2 * at + side]))
+    for copy in copies:
+        copy.start()
+    copies[0].wait()
+    copies[1].wait()
+    table_ref[...] = packed_weights(e_ref, w_ref)
+    for at, out in enumerate((first_ref, second_ref)):
+        block = pl.ds(pl.multiple_of(core * 2 * count + at * count, count), count)
+        out[:, 2 * width :] = table_ref[block, :].astype(BF)
+    for copy in copies[2:]:
+        copy.wait()
+
+
+def prepare(x, cot, expert, weight):
+    rows, width = x.shape
+    shape = jax.ShapeDtypeStruct((rows // 4, 2 * width + rows), BF)
+    return pl.pallas_call(
+        prep_kernel,
+        out_shape=[shape] * 2,
+        in_specs=[HB] * 4,
+        out_specs=[VM] * 2,
+        scratch_shapes=[
+            pltpu.VMEM(expert.shape, jnp.int32),
+            pltpu.VMEM(weight.shape, F32),
+            pltpu.VMEM((rows, rows), F32),
+            pltpu.SemaphoreType.DMA((6,)),
+        ],
+        compiler_params=grant(8),
+        name="prep",
+    )(*in_hbm(x, cot, expert, weight))
+
+
+def start_all(sources, targets, sems):
+    copies = [
+        pltpu.make_async_copy(source, target, sems.at[at])
+        for at, (source, target) in enumerate(zip(sources, targets))
+    ]
+    for copy in copies:
+        copy.start()
+    return copies
+
+
+def wait_for(copies, at):
+    if copies:
+        copies[at].wait()
+
+
+def through_expert(core, half, x_ref, mix_ref, weights, ready, hid_ref, dg_ref, du_ref, mine_ref, theirs_ref, acc_ref):
+    gate_ref, up_ref, down_ref = weights
+    wait_for(ready, 0)
+    gate = nn(x_ref[...], gate_ref[...])
+    sigmoid = 1.0 / (1.0 + jnp.exp(-gate))
+    active = gate * sigmoid
+    wait_for(ready, 1)
+    upper = nn(x_ref[...], up_ref[...])
+    hid_ref[...] = (active * upper).astype(BF)
+    wait_for(ready, 2)
+    d_hidden = nt(mix_ref[...], down_ref[...])
+    du_ref[...] = (d_hidden * active).astype(BF)
+    dg_ref[...] = (d_hidden * upper * sigmoid * (1.0 + gate * (1.0 - sigmoid))).astype(BF)
+    acc_ref[...] = nt(dg_ref[...], gate_ref[...]) + nt(du_ref[...], up_ref[...])
+    for chunk in range(mine_ref.shape[0]):
+        start = pl.multiple_of((2 * chunk + core) * half, half)
+        mine_ref[chunk] = acc_ref[pl.ds(start, half), :]
+        start = pl.multiple_of((2 * chunk + 1 - core) * half, half)
+        theirs_ref[chunk] = acc_ref[pl.ds(start, half), :].astype(BF)
+
+
+def own_kernel(x_hbm, cot_hbm, expert_hbm, weight_hbm, gate_hbm, up_hbm, down_hbm, gate_ref, up_ref, down_ref, x_ref, mix_ref, *refs):
+    outs, (acc_ref, cot_ref, e_ref, w_ref, sems) = refs[:5], refs[5:]
+    mine, core, _ = spot()
+    half = x_ref.shape[0] // 2
+    copies = start_all(
+        (expert_hbm, weight_hbm, x_hbm, cot_hbm, gate_hbm, up_hbm, down_hbm),
+        (e_ref, w_ref, x_ref, cot_ref, gate_ref, up_ref, down_ref),
+        sems,
+    )
+    for copy in copies[:4]:
+        copy.wait()
+    column = column_of(packed_weights(e_ref, w_ref), mine)
+    mix_ref[...] = (column * cot_ref[...].astype(F32)).astype(BF)
+    through_expert(core, half, x_ref, mix_ref, (gate_ref, up_ref, down_ref), copies[4:], *outs, acc_ref)
+
+
+def expert_outs(rows, half, width, hidden):
+    chunks = rows // (2 * half)
+    return (
+        [jax.ShapeDtypeStruct((rows, width), BF)] * 2
+        + [jax.ShapeDtypeStruct((rows, hidden), BF)] * 3
+        + [jax.ShapeDtypeStruct((chunks, half, width), F32), jax.ShapeDtypeStruct((chunks, half, width), BF)]
+    )
+
+
+def own_rows(x, cot, expert, weight, gate_w, up_w, down_w):
+    rows, width = x.shape
+    inputs = (x, cot, expert, weight, gate_w, up_w, down_w)
+    return pl.pallas_call(
+        own_kernel,
+        out_shape=[pltpu.VMEM(one.shape, one.dtype) for one in inputs[4:]]
+        + expert_outs(rows, rows // 2, width, gate_w.shape[1]),
+        in_specs=[HB] * 7,
+        out_specs=[VM] * 10,
+        scratch_shapes=[pltpu.VMEM((rows, width), F32)]
+        + [pltpu.VMEM(one.shape, one.dtype) for one in inputs[1:4]]
+        + [pltpu.SemaphoreType.DMA((7,))],
+        compiler_params=grant(10),
+        name="own_rows",
+    )(*in_hbm(*inputs))
+
+
+def came_kernel(half, layout, *refs):
+    pieces = refs[: len(layout)]
+    weights = refs[len(layout) : len(layout) + 3]
+    x_ref, mix_ref, *outs = refs[len(layout) + 3 : len(layout) + 10]
+    (acc_ref,) = refs[len(layout) + 10 :]
+    width = x_ref.shape[1]
+    mine, core, _ = spot()
+    for piece, (chunk, other, at) in zip(pieces, layout):
+        count = piece.shape[0]
+        start = (2 * chunk + (core ^ other)) * half + at * count
+        block = pl.ds(pl.multiple_of(start, count), count)
+        x_ref[block, :] = piece[:, :width]
+        column = column_of(piece[:, 2 * width :].astype(F32), mine)
+        mix_ref[block, :] = (column * piece[:, width : 2 * width].astype(F32)).astype(BF)
+    through_expert(core, half, x_ref, mix_ref, weights, (), *outs, acc_ref)
+
+
+def came_rows(chunks, half, width, pieces, layout, gate_w, up_w, down_w):
+    rows = 2 * half * chunks
+    held = (gate_w, up_w, down_w)
+    return pl.pallas_call(
+        functools.partial(came_kernel, half, layout),
+        out_shape=expert_outs(rows, half, width, gate_w.shape[1]),
+        in_specs=[VM] * len(pieces) + [VM] * 3,
+        out_specs=[VM] * 7,
+        scratch_shapes=[pltpu.VMEM((rows, width), F32)],
+        compiler_params=grant(14),
+    )(*pieces, *in_vmem(*held))
+
+
+def collect_kernel(count, *refs):
+    outs = refs[-count:]
+    for kind, out in enumerate(outs):
+        at = 0
+        for part in refs[kind : len(refs) - count : count]:
+            out[at : at + part.shape[0], :] = part[...]
+            at += part.shape[0]
+
+
+def collect(parts):
+    count = len(parts[0])
+    total = sum(part[0].shape[0] for part in parts)
+    return pl.pallas_call(
+        functools.partial(collect_kernel, count),
+        out_shape=[jax.ShapeDtypeStruct((total, one.shape[1]), one.dtype) for one in parts[0]],
+        in_specs=[VM] * (count * len(parts)),
+        out_specs=[VM] * count,
+        compiler_params=grant(20),
+        name="collect",
+    )(*[one for part in parts for one in part])
+
+
+def transposed_dot(a, b):
+    return lax.dot_general(a, b, (((0,), (0,)), ((), ())), preferred_element_type=F32).astype(BF)
+
+
+def pair_kernel(mine_ref, theirs_ref, *outs):
+    for chunk, out in enumerate(outs):
+        out[...] = (mine_ref[chunk] + theirs_ref[chunk].astype(F32)).astype(BF)
+
+
+def paired(mine, theirs):
+    chunks, half, width = mine.shape
+    return pl.pallas_call(
+        pair_kernel, out_shape=[jax.ShapeDtypeStruct((half, width), BF)] * chunks,
+        in_specs=[VM, VM], out_specs=[VM] * chunks, compiler_params=grant(6),
+    )(mine, theirs)
+
+
+def split_kernel(groups, levels, own_ref, part_ref, *refs):
+    got = refs[: groups - 1]
+    keep_ref = refs[groups - 1]
+    sends = refs[groups:]
+    half = part_ref.shape[0]
+    share = half // levels
+    _, _, level = spot()
+    for mask in range(levels):
+        here = pl.ds(pl.multiple_of((level ^ mask) * share, share), share)
+        total = own_ref[here, :] + part_ref[here, :].astype(F32)
+        for piece in got:
+            total = total + piece[here, :].astype(F32)
+        if mask == 0:
+            keep_ref[...] = total
+        else:
+            sends[mask - 1][...] = total.astype(BF)
+
+
+def join_kernel(cot_ref, keep_ref, *refs):
+    out_ref = refs[-1]
+    _, core, level = spot()
+    share = keep_ref.shape[0]
+    half = cot_ref.shape[0] // 2
+    start = pl.multiple_of(core * half + level * share, share)
+    total = cot_ref[pl.ds(start, share), :].astype(F32) + keep_ref[...]
+    for piece in refs[:-1]:
+        total = total + piece[...].astype(F32)
+    out_ref[...] = total.astype(BF)
+
+
+def cut_kernel(levels, groups, *refs):
+    blocks, (half_ref, *cuts) = refs[:levels], refs[levels:]
+    mine, _, level = spot()
+    share = blocks[0].shape[0]
+    for mask, block in enumerate(blocks):
+        half_ref[pl.ds(pl.multiple_of((level ^ mask) * share, share), share), :] = block[...]
+    slab = half_ref.shape[1] // groups
+    for mask, cut in enumerate(cuts):
+        cut[...] = half_ref[:, pl.ds(pl.multiple_of((mine ^ mask) * slab, slab), slab)]
+
+
+def exact(a, b, contract):
+    return lax.dot_general(
+        a, b, ((contract[:1], contract[1:]), ((), ())), precision=HIGH, preferred_element_type=F32
+    )
+
+
+def grown_kernel(q_ref, k_ref, decay_ref, state_ref, grown_ref, last_ref, scores_ref, turned_ref):
+    spans, heads = scores_ref.shape[:2]
+    at = lax.broadcasted_iota(jnp.int32, (SPAN, SPAN), 0)
+    to = lax.broadcasted_iota(jnp.int32, (SPAN, SPAN), 1)
+    causal = (at >= to).astype(F32)
+    channel = lax.broadcasted_iota(jnp.int32, (1, q_ref.shape[1]), 1) // DK
+    scale = DK ** (-0.5)
+    for span in range(spans):
+        here = slice(span * SPAN, (span + 1) * SPAN)
+        cumulative = exact(causal, decay_ref[here, :], (1, 0))
+        last = cumulative[SPAN - 1 :, :]
+        last_ref[span] = jnp.broadcast_to(last, last_ref.shape[1:])
+        up, down = jnp.exp(cumulative), jnp.exp(-cumulative)
+        ending = jnp.exp(last - cumulative)
+        keys = k_ref[here, :].astype(F32)
+        grown, shrunk = q_ref[here, :].astype(F32) * up, keys * down
+        for kind, value in enumerate((grown, shrunk, keys * ending, scale * up, scale * down, ending)):
+            grown_ref[kind, here, :] = value
+        for head in range(heads):
+            own = jnp.where(channel == head, grown, 0.0)
+            scores_ref[span, head] = scale * exact(own, shrunk, (1, 1)) * causal
+        turned_ref[span] = state_ref[span].T
+
+
+def mix_kernel(first_ref, second_ref, proj_ref, grown_ref, last_ref, mix_ref, local_ref, message_ref, both_ref):
+    _, core, _ = spot()
+    half = first_ref.shape[0]
+    both_ref[pl.ds(pl.multiple_of(core * half, half), half), :] = first_ref[...]
+    both_ref[pl.ds(pl.multiple_of((1 - core) * half, half), half), :] = second_ref[...]
+    mix_ref[...] = nt(both_ref[...], proj_ref[...])
+    spans, value_dim = local_ref.shape[0], local_ref.shape[1]
+    channel = lax.broadcasted_iota(jnp.int32, (1, local_ref.shape[2]), 1) // DK
+    heads = local_ref.shape[2] // DK
+    carry = jnp.zeros(local_ref.shape[1:], F32)
+    total = jnp.zeros((8, local_ref.shape[2]), F32)
+    for span in reversed(range(spans)):
+        here = slice(span * SPAN, (span + 1) * SPAN)
+        query = grown_ref[0, here, :] * (DK ** (-0.5))
+        grads = jnp.concatenate(
+            [mix_ref[here, head * value_dim : (head + 1) * value_dim] for head in range(heads)], 0
+        )
+        queries = jnp.concatenate([jnp.where(channel == head, query, 0.0) for head in range(heads)], 0)
+        local = exact(grads, queries, (0, 0))
+        local_ref[span] = local
+        carry = local + jnp.exp(last_ref[span][:1, :]) * carry
+        total = total + last_ref[span]
+    message_ref[:value_dim, :] = carry
+    message_ref[value_dim:, :] = jnp.exp(total)
+
+
+def within_kernel(mix_ref, v_ref, grown_ref, scores_ref, state_ref, dq_ref, dk_ref, dv_ref):
+    spans, heads = scores_ref.shape[:2]
+    value_dim = v_ref.shape[1] // heads
+    channel = lax.broadcasted_iota(jnp.int32, (1, heads * DK), 1) // DK
+    line = lax.broadcasted_iota(jnp.int32, (heads * DK, 1), 0) // DK
+    at = lax.broadcasted_iota(jnp.int32, (SPAN, SPAN), 0)
+    to = lax.broadcasted_iota(jnp.int32, (SPAN, SPAN), 1)
+    causal = (at >= to).astype(F32)
+    for span in range(spans):
+        here = slice(span * SPAN, (span + 1) * SPAN)
+        query, key = grown_ref[0, here, :], grown_ref[1, here, :]
+        dots = []
+        for head in range(heads):
+            wide = slice(head * value_dim, (head + 1) * value_dim)
+            grads = mix_ref[here, wide]
+            dots.append(exact(grads, v_ref[here, wide].astype(F32), (1, 1)) * causal)
+            dv_ref[here, wide] = exact(scores_ref[span, head], grads, (0, 0))
+        keys = jnp.concatenate([jnp.where(channel == head, key, 0.0) for head in range(heads)], 0)
+        queries = jnp.concatenate([jnp.where(channel == head, query, 0.0) for head in range(heads)], 0)
+        state = jnp.concatenate([jnp.where(line == head, state_ref[span], 0.0) for head in range(heads)], 1)
+        dq = exact(jnp.concatenate(dots, 1), keys, (1, 0)) + exact(mix_ref[here, :], state, (1, 1))
+        dq_ref[here, :] = grown_ref[3, here, :] * dq
+        dk_ref[here, :] = grown_ref[4, here, :] * exact(jnp.concatenate(dots, 0), queries, (0, 0))
+
+
+def final_kernel(groups, *refs):
+    messages = refs[: groups - 1]
+    (q_ref, k_ref, v_ref, grown_ref, last_ref, turned_ref, local_ref, dq_ref, dk_ref, dv_ref) = refs[
+        groups - 1 : groups + 9
+    ]
+    q_out, k_out, v_out, decay_out = refs[groups + 9 :]
+    mine, _, _ = spot()
+    spans, value_dim, channels = local_ref.shape
+    heads = channels // DK
+    channel = lax.broadcasted_iota(jnp.int32, (1, channels), 1) // DK
+    at = lax.broadcasted_iota(jnp.int32, (SPAN, SPAN), 0)
+    to = lax.broadcasted_iota(jnp.int32, (SPAN, SPAN), 1)
+    onward = (at <= to).astype(F32)
+    ending = jnp.zeros((value_dim, channels), F32)
+    for ahead in reversed(range(1, groups)):
+        message = messages[ahead - 1]
+        passed = message[:value_dim, :] + message[value_dim : value_dim + 1, :] * ending
+        ending = jnp.where(mine + ahead < groups, passed, ending)
+    for span in reversed(range(spans)):
+        here = slice(span * SPAN, (span + 1) * SPAN)
+        values = v_ref[here, :].astype(F32)
+        last = jnp.exp(last_ref[span][:1, :])
+        key_end = grown_ref[2, here, :]
+        ends = jnp.concatenate([jnp.where(channel == head, ending, 0.0) for head in range(heads)], 0)
+        through = exact(values, ends, (1, 0))
+        dq = dq_ref[here, :]
+        dk = dk_ref[here, :] + grown_ref[5, here, :] * through
+        for head in range(heads):
+            wide = slice(head * value_dim, (head + 1) * value_dim)
+            own = jnp.where(channel == head, key_end, 0.0)
+            v_out[here, wide] = (dv_ref[here, wide] + exact(own, ending, (1, 1))).astype(BF)
+        tail = last * jnp.sum(turned_ref[span] * ending, axis=0, keepdims=True)
+        tail = tail + jnp.sum(key_end * through, axis=0, keepdims=True)
+        change = q_ref[here, :].astype(F32) * dq - k_ref[here, :].astype(F32) * dk
+        decay_out[here, :] = exact(onward, change, (1, 0)) + tail
+        q_out[here, :] = dq.astype(BF)
+        k_out[here, :] = dk.astype(BF)
+        ending = local_ref[span] + last * ending
+
+
+def proj_kernel(groups, *refs):
+    out_ref, left_ref, right_ref = refs[-3:]
+    _, core, _ = spot()
+    half = refs[0].shape[0]
+    rows = 2 * half
+    for group in range(groups):
+        own, other, saved = refs[3 * group : 3 * group + 3]
+        left_ref[pl.ds(pl.multiple_of(group * rows + core * half, half), half), :] = own[...]
+        left_ref[pl.ds(pl.multiple_of(group * rows + (1 - core) * half, half), half), :] = other[...]
+        right_ref[group * rows : (group + 1) * rows, :] = saved[...]
+    out_ref[...] = lax.dot_general(
+        left_ref[...], right_ref[...], (((0,), (0,)), ((), ())), preferred_element_type=F32
+    )
+
+
+def call(kernel, outs, args, mib, scratch=()):
+    return pl.pallas_call(
+        kernel, out_shape=outs, in_specs=[VM] * len(args), out_specs=[VM] * len(outs),
+        scratch_shapes=scratch, compiler_params=grant(mib),
+    )(*args)
+
+
+def like(*shape, dtype=F32):
+    return jax.ShapeDtypeStruct(shape, dtype)
+
+
+def whole_rows(mesh):
+    return mesh.shape["sp"] == 4 and mesh.shape["tp"] % 2 == 0
+
+
+def by_rows(*args):
+    return rows_on_device(*args)
+
+
+def rows_on_device(
+    moe_input, cotangent, route_expert, route_weight, w_gate, w_up, w_down, out_proj,
+    saved_out, queries, keys, values, log_decay, span_state,
+):
+    rows, width = moe_input.shape
+    half = rows // 2
+    groups = lax.axis_size("sp")
+    lanes = lax.axis_size("tp")
+    levels = lanes // 2
+    share = half // levels
+    mine = lax.axis_index("sp").astype(jnp.int32)
+    lane = lax.axis_index("tp").astype(jnp.int32)
+    gate_w, up_w, down_w = w_gate[0], w_up[0], w_down[0]
+    expert_t, weight_t = route_expert.T, route_weight.T
+
+    first, second = prepare(moe_input, cotangent, expert_t, weight_t)
+    x_first = swap(first, "sp", 1)
+    y_second = swap(second, "sp", 2)
+    x_second = swap(second, "sp", 1)
+    y_first = swap(first, "sp", 2)
+    x_first, y_second, expert_own = lax.optimization_barrier((x_first, y_second, expert_t))
+    d_first = swap(x_first, "sp", 2)
+    d_second = swap(y_second, "sp", 1)
+    gate_w, up_w, down_w, own_x, own_cot, own_hid, own_dg, own_du, own_mine, own_theirs = own_rows(
+        moe_input, cotangent, expert_own, weight_t, gate_w, up_w, down_w
+    )
+    x_second, y_first, own_theirs = lax.optimization_barrier((x_second, y_first, own_theirs))
+    own_part = swap(own_theirs, "tp", 1)
+    near, far = [x_first, x_second, y_first, y_second], [d_first, d_second]
+    near_layout = [(chunk, other, at) for other in range(2) for chunk in range(2) for at in range(2)]
+    far_layout = [(0, other, at) for other in range(2) for at in range(2)]
+    near += [swap(piece, "tp", 1) for piece in near]
+    near_x, near_cot, near_hid, near_dg, near_du, near_mine, near_theirs = came_rows(
+        2, half, width, near, tuple(near_layout), gate_w, up_w, down_w
+    )
+    near_back = paired(near_mine, swap(near_theirs, "tp", 1))
+    far += [swap(piece, "tp", 1) for piece in far]
+    *far, near_one, near_two = lax.optimization_barrier((*far, *near_back))
+    back = [swap(near_one, "sp", 1)]
+    back.append(swap(near_two, "sp", 2))
+    far_x, far_cot, far_hid, far_dg, far_du, far_mine, far_theirs = came_rows(
+        1, half, width, far, tuple(far_layout), gate_w, up_w, down_w
+    )
+    (far_back,) = paired(far_mine, swap(far_theirs, "tp", 1))
+    back.append(swap(far_back, "sp", 3))
+    all_x, all_cot, hid, dg, du = collect(
+        [
+            [own_x, own_cot, own_hid, own_dg, own_du],
+            [near_x, near_cot, near_hid, near_dg, near_du],
+            [far_x, far_cot, far_hid, far_dg, far_du],
+        ]
+    )
+    grad_down = transposed_dot(hid, all_cot)
+    *back, grad_down = lax.optimization_barrier((*back, grad_down))
+    grad_gate = transposed_dot(all_x, dg)
+    small = jax.ShapeDtypeStruct((share, width), BF)
+    keep, *outgoing = pl.pallas_call(
+        functools.partial(split_kernel, groups, levels),
+        out_shape=[jax.ShapeDtypeStruct((share, width), F32)] + [small] * (levels - 1),
+        in_specs=[VM] * (groups + 1), out_specs=[VM] * levels, name="split", compiler_params=grant(6),
+    )(own_mine[0], own_part[0], *back)
+    incoming = []
+    for mask, piece in enumerate(outgoing):
+        incoming.append(swap(piece, "tp", 2 * (mask + 1)))
+    grad_up = transposed_dot(all_x, du)
+    keep, saved_send = lax.optimization_barrier((keep, saved_out))
+    saved_all = [saved_out]
+    for mask in range(1, groups):
+        saved_all.append(swap(saved_send, "sp", mask))
+    *incoming, grad_gate = lax.optimization_barrier((*incoming, grad_gate))
+    (block,) = call(join_kernel, [small], (cotangent, keep, *incoming), 6)
+    blocks = [block]
+    for mask in range(1, levels):
+        blocks.append(swap(block, "tp", 2 * mask))
+    *blocks, grad_up = lax.optimization_barrier((*blocks, grad_up))
+    slab = width // groups
+    this_half, *cuts = call(
+        functools.partial(cut_kernel, levels, groups),
+        [like(half, width, dtype=BF)] + [like(half, slab, dtype=BF)] * groups, blocks, 6,
+    )
+    other_half = swap(this_half, "tp", 1)
+    got_cuts = [cuts[0]]
+    for mask in range(1, groups):
+        got_cuts.append(swap(cuts[mask], "sp", mask))
+
+    channels, value_dim = queries.shape[1], values.shape[1] * DK // queries.shape[1]
+    spans, heads = rows // SPAN, channels // DK
+    grown, last, scores, turned = call(
+        grown_kernel,
+        [like(6, rows, channels), like(spans, 8, channels), like(spans, heads, SPAN, SPAN),
+         like(spans, value_dim, channels)],
+        (queries, keys, log_decay, span_state), 6,
+    )
+    mix, local, message = call(
+        mix_kernel,
+        [like(rows, heads * value_dim), like(spans, value_dim, channels), like(value_dim + 8, channels)],
+        (this_half, other_half, out_proj, grown, last), 8,
+        [pltpu.VMEM((rows, width), BF)],
+    )
+    messages = []
+    for ahead in range(1, groups):
+        messages.append(lax.ppermute(message, "sp", [(i, i - ahead) for i in range(ahead, groups)]))
+    dq, dk, dv = call(
+        within_kernel, [like(rows, channels)] * 2 + [like(rows, heads * value_dim)],
+        (mix, values, grown, scores, span_state), 6,
+    )
+    parts = []
+    for mask in range(groups):
+        parts += [got_cuts[mask], swap(got_cuts[mask], "tp", 1), saved_all[mask]]
+    (grad_proj,) = call(
+        functools.partial(proj_kernel, groups), [like(slab, saved_out.shape[1])], parts, 8,
+        [pltpu.VMEM((groups * rows, slab), BF), pltpu.VMEM((groups * rows, saved_out.shape[1]), BF)],
+    )
+    grad_queries, grad_keys, grad_values, grad_decay = call(
+        functools.partial(final_kernel, groups),
+        [like(rows, channels, dtype=BF)] * 2 + [like(rows, heads * value_dim, dtype=BF), like(rows, channels)],
+        (*messages, queries, keys, values, grown, last, turned, local, dq, dk, dv), 8,
+    )
+    return (
+        grad_gate[None], grad_up[None], grad_down[None], grad_proj,
+        grad_queries, grad_keys, grad_values, grad_decay,
+    )
+
+
 def solution(mesh):
     placed = (
-        P("sp", None),
-        P("sp", None),
-        P("sp", None),
-        P("sp", None),
-        P("sp", None, "tp"),
-        P("sp", None, "tp"),
-        P("sp", "tp", None),
-        P("tp", None),
-        P("sp", "tp"),
-        P("sp", "tp"),
-        P("sp", "tp"),
-        P("sp", "tp"),
-        P("sp", "tp"),
-        P("sp", "tp", None),
+        P("sp", None), P("sp", None), P("sp", None), P("sp", None),
+        P("sp", None, "tp"), P("sp", None, "tp"), P("sp", "tp", None),
+        P("tp", None), P("sp", "tp"), P("sp", "tp"), P("sp", "tp"),
+        P("sp", "tp"), P("sp", "tp"), P("sp", "tp", None),
     )
     return jax.shard_map(
-        on_device,
+        by_rows if whole_rows(mesh) else by_slots,
         mesh=mesh,
         in_specs=placed,
         out_specs=(
-            P("sp", None, "tp"),
-            P("sp", None, "tp"),
-            P("sp", "tp", None),
-            P("sp", "tp"),
-            P("sp", "tp"),
-            P("sp", "tp"),
-            P("sp", "tp"),
-            P("sp", "tp"),
+            P("sp", None, "tp"), P("sp", None, "tp"), P("sp", "tp", None),
+            P("sp", "tp"), P("sp", "tp"), P("sp", "tp"), P("sp", "tp"), P("sp", "tp"),
         ),
         check_vma=False,
     )

time: 275 us -> 94.8 us (0.34)
  waiting for transfers between devices: 95.9 us -> 23.8 us
  local copies, waits for them, and re-layouts: 63.6 us -> 0.03 us
  blocking collectives: 36.4 us -> 0 us
  matrix products: 44.8 us -> 10.6 us
  starting transfers between devices: 4.16 us -> 34.2 us
  Pallas kernels: 0 us -> 25.1 us
  other arithmetic: 14 us -> 0 us
  between operations: 14.4 us -> 0.93 us
    psum x1 -> x0, waiting for transfers between devices: 49.9 us -> none  [on_device(): total = lax.psum(routed.astype(jnp.bfloat16), 'tp').astype(jnp.float32)]
    ppermute x0 -> x38, starting transfers between devices: none -> 34.2 us  [the longest x35 30.3 us: swap(): return lax.ppermute(value, axis, [(i, i ^ mask) for i in range(size)])]
    dot_general x20 -> x3, matrix products: 44.8 us -> 10.6 us  [transposed_dot(): lax.dot_general(a, b, (((0,), (0,)), ((), ())), preferred_element_type=F32)]
    reduce_scatter x2 -> x0, waiting for transfers between devices: 28 us -> none  [the longest x1 18.3 us: on_device(): lax.psum_scatter(input_grad(d_gate, d_upper, gate_weight, up_weight).asty...]
    pallas_call x0 -> x15, Pallas kernels: none -> 25.1 us  [the longest x2 9.83 us: came_rows(): pl.pallas_call(functools.partial(came_kernel, half, layout), out_shape=ex...]
    ppermute x0 -> x38, waiting for transfers between devices: none -> 23.8 us  [the longest x35 20.8 us: swap(): return lax.ppermute(value, axis, [(i, i ^ mask) for i in range(size)])]
    reshape x15 -> x0, local copies, waits for them, and re-layouts: 18.9 us -> none  [the longest x1 4.1 us: on_device(): jnp.concatenate([weighted, blank], axis=0)[owner]]
    all_to_all x2 -> x0, blocking collectives: 18.8 us -> none  [the longest x1 10.7 us: on_device(): lax.all_to_all(part_in, 'sp', split_axis=1, concat_axis=1, tiled=True)]
  transfers between devices with their start and end apart: 6 -> 38, of which waited for: 5 -> 14; matrix products, arithmetic and copies ran while one was open for 25% -> 11% of each run, Pallas kernels for 0% -> 19%
where the time goes in v1:
time: 94.8 us; the launch traced here: 94.6 us
  starting transfers between devices  34.2 us (36%)
  Pallas kernels  25.1 us (26%)
  waiting for transfers between devices  23.8 us (25%)
  matrix products  10.6 us (11%)
    ppermute x35, starting transfers between devices, swap(): return lax.ppermute(value, axis, [(i, i ^ mask) for i in range(size)])  30.3 us
    ppermute x35, waiting for transfers between devices, swap(): return lax.ppermute(value, axis, [(i, i ^ mask) for i in range(size)])  20.8 us
    dot_general x3, matrix products, transposed_dot(): lax.dot_general(a, b, (((0,), (0,)), ((), ())), preferred_element_type=F32)  10.6 us
    pallas_call x2, Pallas kernels, came_rows(): pl.pallas_call(functools.partial(came_kernel, half, layout), out_shape=ex...  9.83 us
    pallas_call x1, Pallas kernels, own_rows(): pl.pallas_call(own_kernel, out_shape=[pltpu.VMEM(one.shape, one.dtype) fo...  7.64 us
    pallas_call x7, Pallas kernels, call(): pl.pallas_call(kernel, out_shape=outs, in_specs=[VM] * len(args), out_spe...  5.59 us
    ppermute x3, starting transfers between devices, rows_on_device(): lax.ppermute(message, 'sp', [(i, i - ahead) for i in range(ahead, groups)])  3.88 us
    ppermute x3, waiting for transfers between devices, rows_on_device(): lax.ppermute(message, 'sp', [(i, i - ahead) for i in range(ahead, groups)])  3 us
  transfers between devices with their start and end apart: 38, of which 14 were waited for; matrix products, arithmetic and copies ran while one was open for 11% of the time, Pallas kernels for 19%

profile of v1, /device:TPU:0, one launch (start us, length us, event | category | flops | bytes accessed | tf_op | source)
XLA Modules:
  0.0 94.6 jit_solution(11979459100513459541)
XLA Ops:
  1.8 3.0 %collective-permute-start = (bf16[32,4224]{1,0:T(8,128)(2,1)S(1)}, bf16[32,4224]{1,0:T(8,128)(2,1)S(1)}, u32[]{:S(2)}, u32[]{:S(2)}) collective-permute-start(bf16[32,4224]{1,0:T(8,128)(2,1)S(1)} %get-tuple-element.91), channel_id=1, source_target_pairs={{0,8},{8,0},{16,24},{24,16},{1,9},{9,1},{17,25},{25,17},{2,10},{10... | collective-permute-start | bytes 811016 | tf_op jit(solution)/shard_map/ppermute | solution.py:297
  4.9 1.5 %collective-permute-start.1 = (bf16[32,4224]{1,0:T(8,128)(2,1)S(1)}, bf16[32,4224]{1,0:T(8,128)(2,1)S(1)}, u32[]{:S(2)}, u32[]{:S(2)}) collective-permute-start(bf16[32,4224]{1,0:T(8,128)(2,1)S(1)} %get-tuple-element.92), channel_id=1, source_target_pairs={{0,16},{8,24},{16,0},{24,8},{1,17},{9,25},{17,1},{25,9},{2,18},{10... | collective-permute-start | bytes 811016 | tf_op jit(solution)/shard_map/ppermute | solution.py:297
  7.0 5.2 %collective-permute-done.refs_0_ = bf16[32,4224]{1,0:T(8,128)(2,1)S(1)} collective-permute-done((bf16[32,4224]{1,0:T(8,128)(2,1)S(1)}, bf16[32,4224]{1,0:T(8,128)(2,1)S(1)}, u32[]{:S(2)}, u32[]{:S(2)}) %collective-permute-start) | collective-permute-done | bytes 270368 | tf_op jit(solution)/shard_map/ppermute | solution.py:297
  12.2 2.0 %collective-permute-done.1.refs_3_ = bf16[32,4224]{1,0:T(8,128)(2,1)S(1)} collective-permute-done((bf16[32,4224]{1,0:T(8,128)(2,1)S(1)}, bf16[32,4224]{1,0:T(8,128)(2,1)S(1)}, u32[]{:S(2)}, u32[]{:S(2)}) %collective-permute-start.1) | collective-permute-done | bytes 270368 | tf_op jit(solution)/shard_map/ppermute | solution.py:297
  14.2 7.6 %own_rows.1 = (bf16[2048,768]{1,0:T(8,128)(2,1)S(1)}, bf16[2048,768]{1,0:T(8,128)(2,1)S(1)}, bf16[768,2048]{1,0:T(8,128)(2,1)S(1)}, bf16[128,2048]{1,0:T(8,128)(...) custom-call(bf16[128,2048]{1,0:T(8,128)(2,1)} %x_hbm.1, ...), custom_call_target="tpu_custom_call" | custom-call | tf_op jit(solution)/shard_map/own_rows/pallas_call | solution.py:445
  23.0 1.5 %collective-permute-start.5 = (bf16[32,4224]{1,0:T(8,128)(2,1)S(1)}, bf16[32,4224]{1,0:T(8,128)(2,1)S(1)}, u32[]{:S(2)}, u32[]{:S(2)}) collective-permute-start(bf16[32,4224]{1,0:T(8,128)(2,1)S(1)} %collective-permute-done.refs_0_), channel_id=1, source_target_pairs={{0,16},{8,24},{16,0},{24,8},{1,17},{9,25},{17,1},{25,9},{2,18},{10... | collective-permute-start | bytes 811016 | tf_op jit(solution)/shard_map/ppermute | solution.py:297
  25.0 5.3 %shard_map.197 = (bf16[256,2048]{1,0:T(8,128)(2,1)S(1)}, bf16[256,2048]{1,0:T(8,128)(2,1)S(1)}, bf16[256,768]{1,0:T(8,128)(2,1)S(1)}, bf16[256,768]{1,0:T(8,128)...) custom-call(bf16[32,4224]{1,0:T(8,128)(2,1)S(1)} %collective-permute-done.refs, ...), custom_call_target="tpu_custom_call" | custom-call | tf_op jit(solution)/shard_map/pallas_call | solution.py:479
  34.2 4.5 %shard_map.199 = (bf16[128,2048]{1,0:T(8,128)(2,1)S(1)}, bf16[128,2048]{1,0:T(8,128)(2,1)S(1)}, bf16[128,768]{1,0:T(8,128)(2,1)S(1)}, bf16[128,768]{1,0:T(8,128)...) custom-call(bf16[32,4224]{1,0:T(8,128)(2,1)S(1)} %collective-permute-done.5.re, ...), custom_call_target="tpu_custom_call" | custom-call | tf_op jit(solution)/shard_map/pallas_call | solution.py:479
  41.4 2.2 %collective-permute-start.17 = (bf16[64,2048]{1,0:T(8,128)(2,1)S(1)}, bf16[64,2048]{1,0:T(8,128)(2,1)S(1)}, u32[]{:S(2)}, u32[]{:S(2)}) collective-permute-start(bf16[64,2048]{1,0:T(8,128)(2,1)S(1)} %shard_map.200), channel_id=1, source_target_pairs={{0,24},{8,16},{16,8},{24,0},{1,25},{9,17},{17,9},{25,1},{2,26},{10... | collective-permute-start | bytes 786440 | tf_op jit(solution)/shard_map/ppermute | solution.py:297
  43.5 3.5 %convolution_convert_fusion.2 = bf16[768,2048]{1,0:T(8,128)(2,1)} fusion(bf16[512,768]{1,0:T(8,128)(2,1)S(1)} %get-tuple-element.131, bf16[512,2048]{1,0:T(8,128)(2,1)S(1)} %get-tuple-element.132), kind=kOutput, calls=%fused_computation.2 | convolution fusion | flops 1612185600 | bytes 6029312 | tf_op jit(solution)/shard_map/dot_general | solution.py:512
  47.0 1.4 %collective-permute-done.14.refs_0_ = bf16[64,2048]{1,0:T(8,128)(2,1)S(1)} collective-permute-done((bf16[64,2048]{1,0:T(8,128)(2,1)S(1)}, bf16[64,2048]{1,0:T(8,128)(2,1)S(1)}, u32[]{:S(2)}, u32[]{:S(2)}) %collective-permute-start.14) | collective-permute-done | bytes 262176 | tf_op jit(solution)/shard_map/ppermute | solution.py:297
  48.7 4.9 %collective-permute-done.17.refs_2_ = bf16[64,2048]{1,0:T(8,128)(2,1)S(1)} collective-permute-done((bf16[64,2048]{1,0:T(8,128)(2,1)S(1)}, bf16[64,2048]{1,0:T(8,128)(2,1)S(1)}, u32[]{:S(2)}, u32[]{:S(2)}) %collective-permute-start.17) | collective-permute-done | bytes 262176 | tf_op jit(solution)/shard_map/ppermute | solution.py:297
  53.7 1.6 %collective-permute-start.18 = (bf16[16,2048]{1,0:T(8,128)(2,1)S(1)}, bf16[16,2048]{1,0:T(8,128)(2,1)S(1)}, u32[]{:S(2)}, u32[]{:S(2)}) collective-permute-start(bf16[16,2048]{1,0:T(8,128)(2,1)S(1)} %get-tuple-element.136), channel_id=1, source_target_pairs={{0,2},{1,3},{2,0},{3,1},{4,6},{5,7},{6,4},{7,5},{8,10},{9,11},{10,... | collective-permute-start | bytes 196616 | tf_op jit(solution)/shard_map/ppermute | solution.py:297
  55.4 2.6 %collective-permute-start.19 = (bf16[16,2048]{1,0:T(8,128)(2,1)S(1)}, bf16[16,2048]{1,0:T(8,128)(2,1)S(1)}, u32[]{:S(2)}, u32[]{:S(2)}) collective-permute-start(bf16[16,2048]{1,0:T(8,128)(2,1)S(1)} %get-tuple-element.137), channel_id=1, source_target_pairs={{0,4},{1,5},{2,6},{3,7},{4,0},{5,1},{6,2},{7,3},{8,12},{9,13},{10,... | collective-permute-start | bytes 196616 | tf_op jit(solution)/shard_map/ppermute | solution.py:297
  58.2 3.5 %convolution_convert_fusion.1 = bf16[2048,768]{1,0:T(8,128)(2,1)} fusion(bf16[512,2048]{1,0:T(8,128)(2,1)S(1)} %get-tuple-element.139, bf16[512,768]{1,0:T(8,128)(2,1)S(1)} %get-tuple-element.140), kind=kOutput, calls=%fused_computation.1 | convolution fusion | flops 1612185600 | bytes 6029312 | tf_op jit(solution)/shard_map/dot_general | solution.py:512
  62.1 2.0 %collective-permute-done.20.refs_2_ = bf16[16,2048]{1,0:T(8,128)(2,1)S(1)} collective-permute-done((bf16[16,2048]{1,0:T(8,128)(2,1)S(1)}, bf16[16,2048]{1,0:T(8,128)(2,1)S(1)}, u32[]{:S(2)}, u32[]{:S(2)}) %collective-permute-start.20) | collective-permute-done | bytes 65568 | tf_op jit(solution)/shard_map/ppermute | solution.py:297
  64.2 1.9 %collective-permute-start.22 = (bf16[16,2048]{1,0:T(8,128)(2,1)S(1)}, bf16[16,2048]{1,0:T(8,128)(2,1)S(1)}, u32[]{:S(2)}, u32[]{:S(2)}) collective-permute-start(bf16[16,2048]{1,0:T(8,128)(2,1)S(1)} %shard_map.201.refs_0_), channel_id=1, source_target_pairs={{0,4},{1,5},{2,6},{3,7},{4,0},{5,1},{6,2},{7,3},{8,12},{9,13},{10,... | collective-permute-start | bytes 196616 | tf_op jit(solution)/shard_map/ppermute | solution.py:297
  66.1 2.5 %collective-permute-start.23 = (bf16[16,2048]{1,0:T(8,128)(2,1)S(1)}, bf16[16,2048]{1,0:T(8,128)(2,1)S(1)}, u32[]{:S(2)}, u32[]{:S(2)}) collective-permute-start(bf16[16,2048]{1,0:T(8,128)(2,1)S(1)} %shard_map.201.refs_0_), channel_id=1, source_target_pairs={{0,6},{1,7},{2,4},{3,5},{4,2},{5,3},{6,0},{7,1},{8,14},{9,15},{10,... | collective-permute-start | bytes 196616 | tf_op jit(solution)/shard_map/ppermute | solution.py:297
  68.6 3.6 %convolution_convert_fusion = bf16[2048,768]{1,0:T(8,128)(2,1)} fusion(bf16[512,2048]{1,0:T(8,128)(2,1)S(1)} %get-tuple-element.139, bf16[512,768]{1,0:T(8,128)(2,1)S(1)} %get-tuple-element.147), kind=kOutput, calls=%fused_computation | convolution fusion | flops 1612185600 | bytes 6029312 | tf_op jit(solution)/shard_map/dot_general | solution.py:512
  72.3 1.6 %collective-permute-start.27 = (bf16[128,256]{1,0:T(8,128)(2,1)S(1)}, bf16[128,256]{1,0:T(8,128)(2,1)S(1)}, u32[]{:S(2)}, u32[]{:S(2)}) collective-permute-start(bf16[128,256]{1,0:T(8,128)(2,1)S(1)} %copy-done.6), channel_id=1, source_target_pairs={{0,8},{8,0},{16,24},{24,16},{1,9},{9,1},{17,25},{25,17},{2,10},{10... | collective-permute-start | bytes 196616 | tf_op jit(solution)/shard_map/ppermute | solution.py:297
  75.6 1.8 %collective-permute-start.33 = (bf16[128,256]{1,0:T(8,128)(2,1)S(1)}, bf16[128,256]{1,0:T(8,128)(2,1)S(1)}, u32[]{:S(2)}, u32[]{:S(2)}) collective-permute-start(bf16[128,256]{1,0:T(8,128)(2,1)S(1)} %copy-done.6), channel_id=1, source_target_pairs={{0,24},{8,16},{16,8},{24,0},{1,25},{9,17},{17,9},{25,1},{2,26},{10... | collective-permute-start | bytes 196616 | tf_op jit(solution)/shard_map/ppermute | solution.py:297
  78.2 1.9 %collective-permute-start.31 = (bf16[64,512]{1,0:T(8,128)(2,1)S(1)}, bf16[64,512]{1,0:T(8,128)(2,1)S(1)}, u32[]{:S(2)}, u32[]{:S(2)}) collective-permute-start(bf16[64,512]{1,0:T(8,128)(2,1)S(1)} %get-tuple-element.158), channel_id=1, source_target_pairs={{0,24},{8,16},{16,8},{24,0},{1,25},{9,17},{17,9},{25,1},{2,26},{10... | collective-permute-start | bytes 196616 | tf_op jit(solution)/shard_map/ppermute | solution.py:297
  90.2 3.0 %collective-permute-done.37.refs_2_ = f32[136,128]{1,0:T(8,128)S(1)} collective-permute-done((f32[136,128]{1,0:T(8,128)S(1)}, f32[136,128]{1,0:T(8,128)S(1)}, u32[]{:S(2)}, u32[]{:S(2)}) %collective-permute-start.37) | collective-permute-done | bytes 69664 | tf_op jit(solution)/shard_map/ppermute | solution.py:825
  93.2 1.4 %shard_map.207 = (bf16[128,128]{1,0:T(8,128)(2,1)}, bf16[128,128]{1,0:T(8,128)(2,1)}, bf16[128,256]{1,0:T(8,128)(2,1)}, f32[128,128]{1,0:T(8,128)}) custom-call(f32[136,128]{1,0:T(8,128)S(1)} %collective-permute-done.35.refs_0_, f32[136,128]{1,0:T(8,128)S(1)} %collective-permute-done.36.refs_1_, f32[136,128]{1,0:T(8,128)S(1)} %collective-permute-done.37.refs_2_, ...), custom_call_target="tpu_custom_call" | custom-call | tf_op jit(solution)/shard_map/pallas_call | solution.py:706
  (86 shorter events, 23.4 us)
Async XLA Ops:
  1.8 10.4 %collective-permute-start = (bf16[32,4224]{1,0:T(8,128)(2,1)S(1)}, bf16[32,4224]{1,0:T(8,128)(2,1)S(1)}, u32[]{:S(2)}, u32[]{:S(2)}) collective-permute-start(bf16[32,4224]{1,0:T(8,128)(2,1)S(1)} %get-tuple-element.91), channel_id=1, source_target_pairs={{0,8},{8,0},{16,24},{24,16},{1,9},{9,1},{17,25},{25,17},{2,10},{10... | collective-permute-start | bytes 811016 | tf_op jit(solution)/shard_map/ppermute | solution.py:297
  4.9 9.4 %collective-permute-start.1 = (bf16[32,4224]{1,0:T(8,128)(2,1)S(1)}, bf16[32,4224]{1,0:T(8,128)(2,1)S(1)}, u32[]{:S(2)}, u32[]{:S(2)}) collective-permute-start(bf16[32,4224]{1,0:T(8,128)(2,1)S(1)} %get-tuple-element.92), channel_id=1, source_target_pairs={{0,16},{8,24},{16,0},{24,8},{1,17},{9,25},{17,1},{25,9},{2,18},{10... | collective-permute-start | bytes 811016 | tf_op jit(solution)/shard_map/ppermute | solution.py:297
  6.4 15.5 %collective-permute-start.2 = (bf16[32,4224]{1,0:T(8,128)(2,1)S(1)}, bf16[32,4224]{1,0:T(8,128)(2,1)S(1)}, u32[]{:S(2)}, u32[]{:S(2)}) collective-permute-start(bf16[32,4224]{1,0:T(8,128)(2,1)S(1)} %get-tuple-element.92), channel_id=1, source_target_pairs={{0,8},{8,0},{16,24},{24,16},{1,9},{9,1},{17,25},{25,17},{2,10},{10... | collective-permute-start | bytes 811016 | tf_op jit(solution)/shard_map/ppermute | solution.py:297
  6.9 15.0 %collective-permute-start.3 = (bf16[32,4224]{1,0:T(8,128)(2,1)S(1)}, bf16[32,4224]{1,0:T(8,128)(2,1)S(1)}, u32[]{:S(2)}, u32[]{:S(2)}) collective-permute-start(bf16[32,4224]{1,0:T(8,128)(2,1)S(1)} %get-tuple-element.91), channel_id=1, source_target_pairs={{0,16},{8,24},{16,0},{24,8},{1,17},{9,25},{17,1},{25,9},{2,18},{10... | collective-permute-start | bytes 811016 | tf_op jit(solution)/shard_map/ppermute | solution.py:297
  23.0 8.5 %collective-permute-start.5 = (bf16[32,4224]{1,0:T(8,128)(2,1)S(1)}, bf16[32,4224]{1,0:T(8,128)(2,1)S(1)}, u32[]{:S(2)}, u32[]{:S(2)}) collective-permute-start(bf16[32,4224]{1,0:T(8,128)(2,1)S(1)} %collective-permute-done.refs_0_), channel_id=1, source_target_pairs={{0,16},{8,24},{16,0},{24,8},{1,17},{9,25},{17,1},{25,9},{2,18},{10... | collective-permute-start | bytes 811016 | tf_op jit(solution)/shard_map/ppermute | solution.py:297
  24.5 8.2 %collective-permute-start.6 = (bf16[32,4224]{1,0:T(8,128)(2,1)S(1)}, bf16[32,4224]{1,0:T(8,128)(2,1)S(1)}, u32[]{:S(2)}, u32[]{:S(2)}) collective-permute-start(bf16[32,4224]{1,0:T(8,128)(2,1)S(1)} %collective-permute-done.1.refs_3_), channel_id=1, source_target_pairs={{0,8},{8,0},{16,24},{24,16},{1,9},{9,1},{17,25},{25,17},{2,10},{10... | collective-permute-start | bytes 811016 | tf_op jit(solution)/shard_map/ppermute | solution.py:297
  38.9 14.6 %collective-permute-start.4 = (bf16[1,64,2048]{2,1,0:T(8,128)(2,1)S(1)}, bf16[1,64,2048]{2,1,0:T(8,128)(2,1)S(1)}, u32[]{:S(2)}, u32[]{:S(2)}) collective-permute-start(bf16[1,64,2048]{2,1,0:T(8,128)(2,1)S(1)} %get-tuple-element.96), channel_id=1, source_target_pairs={{0,1},{1,0},{2,3},{3,2},{4,5},{5,4},{6,7},{7,6},{8,9},{9,8},{10,11... | collective-permute-start | bytes 786440 | tf_op jit(solution)/shard_map/ppermute | solution.py:297
  39.3 9.2 %collective-permute-start.14 = (bf16[64,2048]{1,0:T(8,128)(2,1)S(1)}, bf16[64,2048]{1,0:T(8,128)(2,1)S(1)}, u32[]{:S(2)}, u32[]{:S(2)}) collective-permute-start(bf16[64,2048]{1,0:T(8,128)(2,1)S(1)} %get-tuple-element.108), channel_id=1, source_target_pairs={{0,8},{8,0},{16,24},{24,16},{1,9},{9,1},{17,25},{25,17},{2,10},{10... | collective-permute-start | bytes 786440 | tf_op jit(solution)/shard_map/ppermute | solution.py:297
  39.8 8.9 %collective-permute-start.15 = (bf16[64,2048]{1,0:T(8,128)(2,1)S(1)}, bf16[64,2048]{1,0:T(8,128)(2,1)S(1)}, u32[]{:S(2)}, u32[]{:S(2)}) collective-permute-start(bf16[64,2048]{1,0:T(8,128)(2,1)S(1)} %get-tuple-element.109), channel_id=1, source_target_pairs={{0,16},{8,24},{16,0},{24,8},{1,17},{9,25},{17,1},{25,9},{2,18},{10... | collective-permute-start | bytes 786440 | tf_op jit(solution)/shard_map/ppermute | solution.py:297
  41.4 12.2 %collective-permute-start.17 = (bf16[64,2048]{1,0:T(8,128)(2,1)S(1)}, bf16[64,2048]{1,0:T(8,128)(2,1)S(1)}, u32[]{:S(2)}, u32[]{:S(2)}) collective-permute-start(bf16[64,2048]{1,0:T(8,128)(2,1)S(1)} %shard_map.200), channel_id=1, source_target_pairs={{0,24},{8,16},{16,8},{24,0},{1,25},{9,17},{17,9},{25,1},{2,26},{10... | collective-permute-start | bytes 786440 | tf_op jit(solution)/shard_map/ppermute | solution.py:297
  53.7 8.0 %collective-permute-start.18 = (bf16[16,2048]{1,0:T(8,128)(2,1)S(1)}, bf16[16,2048]{1,0:T(8,128)(2,1)S(1)}, u32[]{:S(2)}, u32[]{:S(2)}) collective-permute-start(bf16[16,2048]{1,0:T(8,128)(2,1)S(1)} %get-tuple-element.136), channel_id=1, source_target_pairs={{0,2},{1,3},{2,0},{3,1},{4,6},{5,7},{6,4},{7,5},{8,10},{9,11},{10,... | collective-permute-start | bytes 196616 | tf_op jit(solution)/shard_map/ppermute | solution.py:297
  55.4 6.7 %collective-permute-start.19 = (bf16[16,2048]{1,0:T(8,128)(2,1)S(1)}, bf16[16,2048]{1,0:T(8,128)(2,1)S(1)}, u32[]{:S(2)}, u32[]{:S(2)}) collective-permute-start(bf16[16,2048]{1,0:T(8,128)(2,1)S(1)} %get-tuple-element.137), channel_id=1, source_target_pairs={{0,4},{1,5},{2,6},{3,7},{4,0},{5,1},{6,2},{7,3},{8,12},{9,13},{10,... | collective-permute-start | bytes 196616 | tf_op jit(solution)/shard_map/ppermute | solution.py:297
  64.1 8.0 %collective-permute-start.21 = (bf16[16,2048]{1,0:T(8,128)(2,1)S(1)}, bf16[16,2048]{1,0:T(8,128)(2,1)S(1)}, u32[]{:S(2)}, u32[]{:S(2)}) collective-permute-start(bf16[16,2048]{1,0:T(8,128)(2,1)S(1)} %shard_map.201.refs_0_), channel_id=1, source_target_pairs={{0,2},{1,3},{2,0},{3,1},{4,6},{5,7},{6,4},{7,5},{8,10},{9,11},{10,... | collective-permute-start | bytes 196616 | tf_op jit(solution)/shard_map/ppermute | solution.py:297
  64.2 8.0 %collective-permute-start.22 = (bf16[16,2048]{1,0:T(8,128)(2,1)S(1)}, bf16[16,2048]{1,0:T(8,128)(2,1)S(1)}, u32[]{:S(2)}, u32[]{:S(2)}) collective-permute-start(bf16[16,2048]{1,0:T(8,128)(2,1)S(1)} %shard_map.201.refs_0_), channel_id=1, source_target_pairs={{0,4},{1,5},{2,6},{3,7},{4,0},{5,1},{6,2},{7,3},{8,12},{9,13},{10,... | collective-permute-start | bytes 196616 | tf_op jit(solution)/shard_map/ppermute | solution.py:297
  66.1 6.1 %collective-permute-start.23 = (bf16[16,2048]{1,0:T(8,128)(2,1)S(1)}, bf16[16,2048]{1,0:T(8,128)(2,1)S(1)}, u32[]{:S(2)}, u32[]{:S(2)}) collective-permute-start(bf16[16,2048]{1,0:T(8,128)(2,1)S(1)} %shard_map.201.refs_0_), channel_id=1, source_target_pairs={{0,6},{1,7},{2,4},{3,5},{4,2},{5,3},{6,0},{7,1},{8,14},{9,15},{10,... | collective-permute-start | bytes 196616 | tf_op jit(solution)/shard_map/ppermute | solution.py:297
  72.2 7.9 %collective-permute-start.34 = (bf16[64,2048]{1,0:T(8,128)(2,1)S(1)}, bf16[64,2048]{1,0:T(8,128)(2,1)S(1)}, u32[]{:S(2)}, u32[]{:S(2)}) collective-permute-start(bf16[64,2048]{1,0:T(8,128)(2,1)S(1)} %get-tuple-element.159.first_ref), channel_id=1, source_target_pairs={{0,1},{1,0},{2,3},{3,2},{4,5},{5,4},{6,7},{7,6},{8,9},{9,8},{10,11... | collective-permute-start | bytes 786440 | tf_op jit(solution)/shard_map/ppermute | solution.py:297
  75.6 6.7 %collective-permute-start.33 = (bf16[128,256]{1,0:T(8,128)(2,1)S(1)}, bf16[128,256]{1,0:T(8,128)(2,1)S(1)}, u32[]{:S(2)}, u32[]{:S(2)}) collective-permute-start(bf16[128,256]{1,0:T(8,128)(2,1)S(1)} %copy-done.6), channel_id=1, source_target_pairs={{0,24},{8,16},{16,8},{24,0},{1,25},{9,17},{17,9},{25,1},{2,26},{10... | collective-permute-start | bytes 196616 | tf_op jit(solution)/shard_map/ppermute | solution.py:297
  77.4 6.2 %collective-permute-start.28 = (bf16[64,512]{1,0:T(8,128)(2,1)S(1)}, bf16[64,512]{1,0:T(8,128)(2,1)S(1)}, u32[]{:S(2)}, u32[]{:S(2)}) collective-permute-start(bf16[64,512]{1,0:T(8,128)(2,1)S(1)} %get-tuple-element.157), channel_id=1, source_target_pairs={{0,16},{8,24},{16,0},{24,8},{1,17},{9,25},{17,1},{25,9},{2,18},{10... | collective-permute-start | bytes 196616 | tf_op jit(solution)/shard_map/ppermute | solution.py:297
  78.2 6.7 %collective-permute-start.31 = (bf16[64,512]{1,0:T(8,128)(2,1)S(1)}, bf16[64,512]{1,0:T(8,128)(2,1)S(1)}, u32[]{:S(2)}, u32[]{:S(2)}) collective-permute-start(bf16[64,512]{1,0:T(8,128)(2,1)S(1)} %get-tuple-element.158), channel_id=1, source_target_pairs={{0,24},{8,16},{16,8},{24,0},{1,25},{9,17},{17,9},{25,1},{2,26},{10... | collective-permute-start | bytes 196616 | tf_op jit(solution)/shard_map/ppermute | solution.py:297
  80.2 6.1 %collective-permute-start.24 = (bf16[64,512]{1,0:T(8,128)(2,1)S(1)}, bf16[64,512]{1,0:T(8,128)(2,1)S(1)}, u32[]{:S(2)}, u32[]{:S(2)}) collective-permute-start(bf16[64,512]{1,0:T(8,128)(2,1)S(1)} %get-tuple-element.154.refs_0_), channel_id=1, source_target_pairs={{0,1},{1,0},{2,3},{3,2},{4,5},{5,4},{6,7},{7,6},{8,9},{9,8},{10,11... | collective-permute-start | bytes 196616 | tf_op jit(solution)/shard_map/ppermute | solution.py:297
  80.2 6.2 %collective-permute-start.26 = (bf16[64,512]{1,0:T(8,128)(2,1)S(1)}, bf16[64,512]{1,0:T(8,128)(2,1)S(1)}, u32[]{:S(2)}, u32[]{:S(2)}) collective-permute-start(bf16[64,512]{1,0:T(8,128)(2,1)S(1)} %collective-permute-done.25.refs_3_), channel_id=1, source_target_pairs={{0,1},{1,0},{2,3},{3,2},{4,5},{5,4},{6,7},{7,6},{8,9},{9,8},{10,11... | collective-permute-start | bytes 196616 | tf_op jit(solution)/shard_map/ppermute | solution.py:297
  82.3 7.9 %collective-permute-start.35 = (f32[136,128]{1,0:T(8,128)S(1)}, f32[136,128]{1,0:T(8,128)S(1)}, u32[]{:S(2)}, u32[]{:S(2)}) collective-permute-start(f32[136,128]{1,0:T(8,128)S(1)} %get-tuple-element.162), channel_id=1, source_target_pairs={{8,0},{16,8},{24,16},{9,1},{17,9},{25,17},{10,2},{18,10},{26,18},{... | collective-permute-start | bytes 208904 | tf_op jit(solution)/shard_map/ppermute | solution.py:825
  83.6 6.6 %collective-permute-start.36 = (f32[136,128]{1,0:T(8,128)S(1)}, f32[136,128]{1,0:T(8,128)S(1)}, u32[]{:S(2)}, u32[]{:S(2)}) collective-permute-start(f32[136,128]{1,0:T(8,128)S(1)} %get-tuple-element.162), channel_id=1, source_target_pairs={{16,0},{24,8},{17,1},{25,9},{18,2},{26,10},{19,3},{27,11},{20,4},{... | collective-permute-start | bytes 208904 | tf_op jit(solution)/shard_map/ppermute | solution.py:825
  84.9 8.3 %collective-permute-start.37 = (f32[136,128]{1,0:T(8,128)S(1)}, f32[136,128]{1,0:T(8,128)S(1)}, u32[]{:S(2)}, u32[]{:S(2)}) collective-permute-start(f32[136,128]{1,0:T(8,128)S(1)} %get-tuple-element.162), channel_id=1, source_target_pairs={{24,0},{25,1},{26,2},{27,3},{28,4},{29,5},{30,6},{31,7}} | collective-permute-start | bytes 208904 | tf_op jit(solution)/shard_map/ppermute | solution.py:825
  (22 other events, 130.1 us)

commit v2 on v1

--- a/solution.py
+++ b/solution.py
@@ -606,7 +606,7 @@
     channel = lax.broadcasted_iota(jnp.int32, (1, local_ref.shape[2]), 1) // DK
     heads = local_ref.shape[2] // DK
     carry = jnp.zeros(local_ref.shape[1:], F32)
-    total = jnp.zeros((8, local_ref.shape[2]), F32)
+    total = jnp.zeros((16, local_ref.shape[2]), F32)
     for span in reversed(range(spans)):
         here = slice(span * SPAN, (span + 1) * SPAN)
         query = grown_ref[0, here, :] * (DK ** (-0.5))
@@ -618,8 +618,8 @@
         local_ref[span] = local
         carry = local + jnp.exp(last_ref[span][:1, :]) * carry
         total = total + last_ref[span]
-    message_ref[:value_dim, :] = carry
-    message_ref[value_dim:, :] = jnp.exp(total)
+    message_ref[:value_dim, :] = carry.astype(BF)
+    message_ref[value_dim:, :] = jnp.exp(total).astype(BF)
 
 
 def within_kernel(mix_ref, v_ref, grown_ref, scores_ref, state_ref, dq_ref, dk_ref, dv_ref):
@@ -662,7 +662,7 @@
     onward = (at <= to).astype(F32)
     ending = jnp.zeros((value_dim, channels), F32)
     for ahead in reversed(range(1, groups)):
-        message = messages[ahead - 1]
+        message = messages[ahead - 1][...].astype(F32)
         passed = message[:value_dim, :] + message[value_dim : value_dim + 1, :] * ending
         ending = jnp.where(mine + ahead < groups, passed, ending)
     for span in reversed(range(spans)):
@@ -741,14 +741,24 @@
     y_second = swap(second, "sp", 2)
     x_second = swap(second, "sp", 1)
     y_first = swap(first, "sp", 2)
-    x_first, y_second, expert_own = lax.optimization_barrier((x_first, y_second, expert_t))
+    gate_w, up_w, down_w, own_x, own_cot, own_hid, own_dg, own_du, own_mine, own_theirs = own_rows(
+        moe_input, cotangent, expert_t, weight_t, gate_w, up_w, down_w
+    )
+    x_first, y_second, own_theirs, queries_then = lax.optimization_barrier(
+        (x_first, y_second, own_theirs, queries)
+    )
     d_first = swap(x_first, "sp", 2)
     d_second = swap(y_second, "sp", 1)
-    gate_w, up_w, down_w, own_x, own_cot, own_hid, own_dg, own_du, own_mine, own_theirs = own_rows(
-        moe_input, cotangent, expert_own, weight_t, gate_w, up_w, down_w
-    )
-    x_second, y_first, own_theirs = lax.optimization_barrier((x_second, y_first, own_theirs))
     own_part = swap(own_theirs, "tp", 1)
+    channels, value_dim = queries.shape[1], values.shape[1] * DK // queries.shape[1]
+    spans, heads = rows // SPAN, channels // DK
+    grown, last, scores, turned = call(
+        grown_kernel,
+        [like(6, rows, channels), like(spans, 16, channels), like(spans, heads, SPAN, SPAN),
+         like(spans, value_dim, channels)],
+        (queries_then, keys, log_decay, span_state), 6,
+    )
+    x_second, y_first, grown = lax.optimization_barrier((x_second, y_first, grown))
     near, far = [x_first, x_second, y_first, y_second], [d_first, d_second]
     near_layout = [(chunk, other, at) for other in range(2) for chunk in range(2) for at in range(2)]
     far_layout = [(0, other, at) for other in range(2) for at in range(2)]
@@ -756,7 +766,8 @@
     near_x, near_cot, near_hid, near_dg, near_du, near_mine, near_theirs = came_rows(
         2, half, width, near, tuple(near_layout), gate_w, up_w, down_w
     )
-    near_back = paired(near_mine, swap(near_theirs, "tp", 1))
+    near_partner = swap(near_theirs, "tp", 1)
+    near_back = paired(near_mine, near_partner)
     far += [swap(piece, "tp", 1) for piece in far]
     *far, near_one, near_two = lax.optimization_barrier((*far, *near_back))
     back = [swap(near_one, "sp", 1)]
@@ -774,8 +785,8 @@
         ]
     )
     grad_down = transposed_dot(hid, all_cot)
-    *back, grad_down = lax.optimization_barrier((*back, grad_down))
     grad_gate = transposed_dot(all_x, dg)
+    *back, grad_down, grad_gate = lax.optimization_barrier((*back, grad_down, grad_gate))
     small = jax.ShapeDtypeStruct((share, width), BF)
     keep, *outgoing = pl.pallas_call(
         functools.partial(split_kernel, groups, levels),
@@ -790,7 +801,6 @@
     saved_all = [saved_out]
     for mask in range(1, groups):
         saved_all.append(swap(saved_send, "sp", mask))
-    *incoming, grad_gate = lax.optimization_barrier((*incoming, grad_gate))
     (block,) = call(join_kernel, [small], (cotangent, keep, *incoming), 6)
     blocks = [block]
     for mask in range(1, levels):
@@ -806,17 +816,9 @@
     for mask in range(1, groups):
         got_cuts.append(swap(cuts[mask], "sp", mask))
 
-    channels, value_dim = queries.shape[1], values.shape[1] * DK // queries.shape[1]
-    spans, heads = rows // SPAN, channels // DK
-    grown, last, scores, turned = call(
-        grown_kernel,
-        [like(6, rows, channels), like(spans, 8, channels), like(spans, heads, SPAN, SPAN),
-         like(spans, value_dim, channels)],
-        (queries, keys, log_decay, span_state), 6,
-    )
     mix, local, message = call(
         mix_kernel,
-        [like(rows, heads * value_dim), like(spans, value_dim, channels), like(value_dim + 8, channels)],
+        [like(rows, heads * value_dim), like(spans, value_dim, channels), like(value_dim + 16, channels, dtype=BF)],
         (this_half, other_half, out_proj, grown, last), 8,
         [pltpu.VMEM((rows, width), BF)],
     )
@@ -827,6 +829,7 @@
         within_kernel, [like(rows, channels)] * 2 + [like(rows, heads * value_dim)],
         (mix, values, grown, scores, span_state), 6,
     )
+    *got_cuts, dq = lax.optimization_barrier((*got_cuts, dq))
     parts = []
     for mask in range(groups):
         parts += [got_cuts[mask], swap(got_cuts[mask], "tp", 1), saved_all[mask]]

time: 94.8 us -> 90.1 us (0.950)
  waiting for transfers between devices: 23.8 us -> 15.9 us
  starting transfers between devices: 34.2 us -> 37.3 us
    ppermute x35, waiting for transfers between devices: 20.8 us -> 15.9 us  [swap(): return lax.ppermute(value, axis, [(i, i ^ mask) for i in range(size)])]
    ppermute x35, starting transfers between devices: 30.3 us -> 33.4 us  [swap(): return lax.ppermute(value, axis, [(i, i ^ mask) for i in range(size)])]
    ppermute x3, waiting for transfers between devices: 3 us -> 0.01 us  [rows_on_device(): lax.ppermute(message, 'sp', [(i, i - ahead) for i in range(ahead, groups)])]
  transfers between devices with their start and end apart: 38 -> 38, of which waited for: 14 -> 9; matrix products, arithmetic and copies ran while one was open for 11% -> 12% of each run, Pallas kernels for 19% -> 25%
where the time goes in v2:
time: 90.1 us; the launch traced here: 89.9 us
  starting transfers between devices  37.3 us (41%)
  Pallas kernels  25.2 us (28%)
  waiting for transfers between devices  15.9 us (18%)
  matrix products  10.6 us (12%)
  between operations  0.92 us (1%)
    ppermute x35, starting transfers between devices, swap(): return lax.ppermute(value, axis, [(i, i ^ mask) for i in range(size)])  33.4 us
    ppermute x35, waiting for transfers between devices, swap(): return lax.ppermute(value, axis, [(i, i ^ mask) for i in range(size)])  15.9 us
    dot_general x3, matrix products, transposed_dot(): lax.dot_general(a, b, (((0,), (0,)), ((), ())), preferred_element_type=F32)  10.6 us
    pallas_call x2, Pallas kernels, came_rows(): pl.pallas_call(functools.partial(came_kernel, half, layout), out_shape=ex...  10 us
    pallas_call x1, Pallas kernels, own_rows(): pl.pallas_call(own_kernel, out_shape=[pltpu.VMEM(one.shape, one.dtype) fo...  7.7 us
    pallas_call x7, Pallas kernels, call(): pl.pallas_call(kernel, out_shape=outs, in_specs=[VM] * len(args), out_spe...  5.6 us
    ppermute x3, starting transfers between devices, rows_on_device(): lax.ppermute(message, 'sp', [(i, i - ahead) for i in range(ahead, groups)])  3.88 us
  transfers between devices with their start and end apart: 38, of which 9 were waited for; matrix products, arithmetic and copies ran while one was open for 12% of the time, Pallas kernels for 25%

profile of v2, /device:TPU:0, one launch (start us, length us, event | category | flops | bytes accessed | tf_op | source)
XLA Modules:
  0.0 89.9 jit_solution(4834880880450400809)
XLA Ops:
  1.8 3.0 %collective-permute-start = (bf16[32,4224]{1,0:T(8,128)(2,1)S(1)}, bf16[32,4224]{1,0:T(8,128)(2,1)S(1)}, u32[]{:S(2)}, u32[]{:S(2)}) collective-permute-start(bf16[32,4224]{1,0:T(8,128)(2,1)S(1)} %get-tuple-element.94), channel_id=1, source_target_pairs={{0,8},{8,0},{16,24},{24,16},{1,9},{9,1},{17,25},{25,17},{2,10},{10... | collective-permute-start | bytes 811016 | tf_op jit(solution)/shard_map/ppermute | solution.py:297
  4.9 1.5 %collective-permute-start.1 = (bf16[32,4224]{1,0:T(8,128)(2,1)S(1)}, bf16[32,4224]{1,0:T(8,128)(2,1)S(1)}, u32[]{:S(2)}, u32[]{:S(2)}) collective-permute-start(bf16[32,4224]{1,0:T(8,128)(2,1)S(1)} %get-tuple-element.95), channel_id=1, source_target_pairs={{0,16},{8,24},{16,0},{24,8},{1,17},{9,25},{17,1},{25,9},{2,18},{10... | collective-permute-start | bytes 811016 | tf_op jit(solution)/shard_map/ppermute | solution.py:297
  7.0 7.7 %own_rows.1 = (bf16[2048,768]{1,0:T(8,128)(2,1)S(1)}, bf16[2048,768]{1,0:T(8,128)(2,1)S(1)}, bf16[768,2048]{1,0:T(8,128)(2,1)S(1)}, bf16[128,2048]{1,0:T(8,128)(...) custom-call(bf16[128,2048]{1,0:T(8,128)(2,1)} %x_hbm.1, ...), custom_call_target="tpu_custom_call" | custom-call | tf_op jit(solution)/shard_map/own_rows/pallas_call | solution.py:445
  15.4 1.7 %collective-permute-done.6.refs_1_ = bf16[32,4224]{1,0:T(8,128)(2,1)S(1)} collective-permute-done((bf16[32,4224]{1,0:T(8,128)(2,1)S(1)}, bf16[32,4224]{1,0:T(8,128)(2,1)S(1)}, u32[]{:S(2)}, u32[]{:S(2)}) %collective-permute-start.6) | collective-permute-done | bytes 270368 | tf_op jit(solution)/shard_map/ppermute | solution.py:297
  17.1 1.5 %collective-permute-done.7.refs_2_ = bf16[32,4224]{1,0:T(8,128)(2,1)S(1)} collective-permute-done((bf16[32,4224]{1,0:T(8,128)(2,1)S(1)}, bf16[32,4224]{1,0:T(8,128)(2,1)S(1)}, u32[]{:S(2)}, u32[]{:S(2)}) %collective-permute-start.7) | collective-permute-done | bytes 270368 | tf_op jit(solution)/shard_map/ppermute | solution.py:297
  19.6 1.5 %collective-permute-start.2 = (bf16[32,4224]{1,0:T(8,128)(2,1)S(1)}, bf16[32,4224]{1,0:T(8,128)(2,1)S(1)}, u32[]{:S(2)}, u32[]{:S(2)}) collective-permute-start(bf16[32,4224]{1,0:T(8,128)(2,1)S(1)} %collective-permute-done.refs_0_), channel_id=1, source_target_pairs={{0,16},{8,24},{16,0},{24,8},{1,17},{9,25},{17,1},{25,9},{2,18},{10... | collective-permute-start | bytes 811016 | tf_op jit(solution)/shard_map/ppermute | solution.py:297
  21.7 5.4 %shard_map.198 = (bf16[256,2048]{1,0:T(8,128)(2,1)S(1)}, bf16[256,2048]{1,0:T(8,128)(2,1)S(1)}, bf16[256,768]{1,0:T(8,128)(2,1)S(1)}, bf16[256,768]{1,0:T(8,128)...) custom-call(bf16[32,4224]{1,0:T(8,128)(2,1)S(1)} %collective-permute-done.refs, ...), custom_call_target="tpu_custom_call" | custom-call | tf_op jit(solution)/shard_map/pallas_call | solution.py:479
  30.8 4.6 %shard_map.200 = (bf16[128,2048]{1,0:T(8,128)(2,1)S(1)}, bf16[128,2048]{1,0:T(8,128)(2,1)S(1)}, bf16[128,768]{1,0:T(8,128)(2,1)S(1)}, bf16[128,768]{1,0:T(8,128)...) custom-call(bf16[32,4224]{1,0:T(8,128)(2,1)S(1)} %collective-permute-done.2.re, ...), custom_call_target="tpu_custom_call" | custom-call | tf_op jit(solution)/shard_map/pallas_call | solution.py:479
  37.5 3.5 %convolution_convert_fusion.1 = bf16[2048,768]{1,0:T(8,128)(2,1)} fusion(bf16[512,2048]{1,0:T(8,128)(2,1)S(1)} %get-tuple-element.135, bf16[512,768]{1,0:T(8,128)(2,1)S(1)} %get-tuple-element.136), kind=kOutput, calls=%fused_computation.1 | convolution fusion | flops 1612185600 | bytes 6029312 | tf_op jit(solution)/shard_map/dot_general | solution.py:512
  41.1 2.1 %collective-permute-start.16 = (bf16[64,2048]{1,0:T(8,128)(2,1)S(1)}, bf16[64,2048]{1,0:T(8,128)(2,1)S(1)}, u32[]{:S(2)}, u32[]{:S(2)}) collective-permute-start(bf16[64,2048]{1,0:T(8,128)(2,1)S(1)} %shard_map.201), channel_id=1, source_target_pairs={{0,24},{8,16},{16,8},{24,0},{1,25},{9,17},{17,9},{25,1},{2,26},{10... | collective-permute-start | bytes 786440 | tf_op jit(solution)/shard_map/ppermute | solution.py:297
  43.2 3.5 %convolution_convert_fusion.2 = bf16[768,2048]{1,0:T(8,128)(2,1)} fusion(bf16[512,768]{1,0:T(8,128)(2,1)S(1)} %get-tuple-element.133, bf16[512,2048]{1,0:T(8,128)(2,1)S(1)} %get-tuple-element.134), kind=kOutput, calls=%fused_computation.2 | convolution fusion | flops 1612185600 | bytes 6029312 | tf_op jit(solution)/shard_map/dot_general | solution.py:512
  46.7 3.5 %collective-permute-done.16.refs_2_ = bf16[64,2048]{1,0:T(8,128)(2,1)S(1)} collective-permute-done((bf16[64,2048]{1,0:T(8,128)(2,1)S(1)}, bf16[64,2048]{1,0:T(8,128)(2,1)S(1)}, u32[]{:S(2)}, u32[]{:S(2)}) %collective-permute-start.16) | collective-permute-done | bytes 262176 | tf_op jit(solution)/shard_map/ppermute | solution.py:297
  50.4 1.6 %collective-permute-start.18 = (bf16[16,2048]{1,0:T(8,128)(2,1)S(1)}, bf16[16,2048]{1,0:T(8,128)(2,1)S(1)}, u32[]{:S(2)}, u32[]{:S(2)}) collective-permute-start(bf16[16,2048]{1,0:T(8,128)(2,1)S(1)} %get-tuple-element.145), channel_id=1, source_target_pairs={{0,2},{1,3},{2,0},{3,1},{4,6},{5,7},{6,4},{7,5},{8,10},{9,11},{10,... | collective-permute-start | bytes 196616 | tf_op jit(solution)/shard_map/ppermute | solution.py:297
  52.0 2.6 %collective-permute-start.19 = (bf16[16,2048]{1,0:T(8,128)(2,1)S(1)}, bf16[16,2048]{1,0:T(8,128)(2,1)S(1)}, u32[]{:S(2)}, u32[]{:S(2)}) collective-permute-start(bf16[16,2048]{1,0:T(8,128)(2,1)S(1)} %get-tuple-element.146), channel_id=1, source_target_pairs={{0,4},{1,5},{2,6},{3,7},{4,0},{5,1},{6,2},{7,3},{8,12},{9,13},{10,... | collective-permute-start | bytes 196616 | tf_op jit(solution)/shard_map/ppermute | solution.py:297
  55.4 3.2 %collective-permute-done.19.refs_1_ = bf16[16,2048]{1,0:T(8,128)(2,1)S(1)} collective-permute-done((bf16[16,2048]{1,0:T(8,128)(2,1)S(1)}, bf16[16,2048]{1,0:T(8,128)(2,1)S(1)}, u32[]{:S(2)}, u32[]{:S(2)}) %collective-permute-start.19) | collective-permute-done | bytes 65568 | tf_op jit(solution)/shard_map/ppermute | solution.py:297
  58.6 2.4 %collective-permute-done.20.refs_2_ = bf16[16,2048]{1,0:T(8,128)(2,1)S(1)} collective-permute-done((bf16[16,2048]{1,0:T(8,128)(2,1)S(1)}, bf16[16,2048]{1,0:T(8,128)(2,1)S(1)}, u32[]{:S(2)}, u32[]{:S(2)}) %collective-permute-start.20) | collective-permute-done | bytes 65568 | tf_op jit(solution)/shard_map/ppermute | solution.py:297
  62.4 3.1 %collective-permute-start.23 = (bf16[16,2048]{1,0:T(8,128)(2,1)S(1)}, bf16[16,2048]{1,0:T(8,128)(2,1)S(1)}, u32[]{:S(2)}, u32[]{:S(2)}) collective-permute-start(bf16[16,2048]{1,0:T(8,128)(2,1)S(1)} %shard_map.202.refs_0_), channel_id=1, source_target_pairs={{0,6},{1,7},{2,4},{3,5},{4,2},{5,3},{6,0},{7,1},{8,14},{9,15},{10,... | collective-permute-start | bytes 196616 | tf_op jit(solution)/shard_map/ppermute | solution.py:297
  65.5 3.5 %convolution_convert_fusion = bf16[2048,768]{1,0:T(8,128)(2,1)} fusion(bf16[512,2048]{1,0:T(8,128)(2,1)S(1)} %get-tuple-element.135, bf16[512,768]{1,0:T(8,128)(2,1)S(1)} %get-tuple-element.148), kind=kOutput, calls=%fused_computation | convolution fusion | flops 1612185600 | bytes 6029312 | tf_op jit(solution)/shard_map/dot_general | solution.py:512
  69.2 1.5 %collective-permute-start.24 = (bf16[64,512]{1,0:T(8,128)(2,1)S(1)}, bf16[64,512]{1,0:T(8,128)(2,1)S(1)}, u32[]{:S(2)}, u32[]{:S(2)}) collective-permute-start(bf16[64,512]{1,0:T(8,128)(2,1)S(1)} %get-tuple-element.156), channel_id=1, source_target_pairs={{0,8},{8,0},{16,24},{24,16},{1,9},{9,1},{17,25},{25,17},{2,10},{10... | collective-permute-start | bytes 196616 | tf_op jit(solution)/shard_map/ppermute | solution.py:297
  72.8 1.4 %collective-permute-start.30 = (bf16[128,256]{1,0:T(8,128)(2,1)S(1)}, bf16[128,256]{1,0:T(8,128)(2,1)S(1)}, u32[]{:S(2)}, u32[]{:S(2)}) collective-permute-start(bf16[128,256]{1,0:T(8,128)(2,1)S(1)} %copy-done.6), channel_id=1, source_target_pairs={{0,8},{8,0},{16,24},{24,16},{1,9},{9,1},{17,25},{25,17},{2,10},{10... | collective-permute-start | bytes 196616 | tf_op jit(solution)/shard_map/ppermute | solution.py:297
  76.2 1.3 %collective-permute-start.35 = (bf16[144,128]{1,0:T(8,128)(2,1)S(1)}, bf16[144,128]{1,0:T(8,128)(2,1)S(1)}, u32[]{:S(2)}, u32[]{:S(2)}) collective-permute-start(bf16[144,128]{1,0:T(8,128)(2,1)S(1)} %get-tuple-element.170), channel_id=1, source_target_pairs={{8,0},{16,8},{24,16},{9,1},{17,9},{25,17},{10,2},{18,10},{26,18},{... | collective-permute-start | bytes 110600 | tf_op jit(solution)/shard_map/ppermute | solution.py:827
  77.5 1.3 %collective-permute-start.36 = (bf16[144,128]{1,0:T(8,128)(2,1)S(1)}, bf16[144,128]{1,0:T(8,128)(2,1)S(1)}, u32[]{:S(2)}, u32[]{:S(2)}) collective-permute-start(bf16[144,128]{1,0:T(8,128)(2,1)S(1)} %get-tuple-element.170), channel_id=1, source_target_pairs={{16,0},{24,8},{17,1},{25,9},{18,2},{26,10},{19,3},{27,11},{20,4},{... | collective-permute-start | bytes 110600 | tf_op jit(solution)/shard_map/ppermute | solution.py:827
  81.4 4.8 %collective-permute-start.34 = (bf16[128,256]{1,0:T(8,128)(2,1)S(1)}, bf16[128,256]{1,0:T(8,128)(2,1)S(1)}, u32[]{:S(2)}, u32[]{:S(2)}) collective-permute-start(bf16[128,256]{1,0:T(8,128)(2,1)S(1)} %copy-done.6), channel_id=1, source_target_pairs={{0,24},{8,16},{16,8},{24,0},{1,25},{9,17},{17,9},{25,1},{2,26},{10... | collective-permute-start | bytes 196616 | tf_op jit(solution)/shard_map/ppermute | solution.py:297
  87.2 1.4 %shard_map.207 = (bf16[128,128]{1,0:T(8,128)(2,1)}, bf16[128,128]{1,0:T(8,128)(2,1)}, bf16[128,256]{1,0:T(8,128)(2,1)}, f32[128,128]{1,0:T(8,128)}) custom-call(bf16[144,128]{1,0:T(8,128)(2,1)S(1)} %collective-permute-done.35.refs_0_, bf16[144,128]{1,0:T(8,128)(2,1)S(1)} %collective-permute-done.36.refs_1_, ...), custom_call_target="tpu_custom_call" | custom-call | tf_op jit(solution)/shard_map/pallas_call | solution.py:706
  (86 shorter events, 21.2 us)
Async XLA Ops:
  1.8 12.9 %collective-permute-start = (bf16[32,4224]{1,0:T(8,128)(2,1)S(1)}, bf16[32,4224]{1,0:T(8,128)(2,1)S(1)}, u32[]{:S(2)}, u32[]{:S(2)}) collective-permute-start(bf16[32,4224]{1,0:T(8,128)(2,1)S(1)} %get-tuple-element.94), channel_id=1, source_target_pairs={{0,8},{8,0},{16,24},{24,16},{1,9},{9,1},{17,25},{25,17},{2,10},{10... | collective-permute-start | bytes 811016 | tf_op jit(solution)/shard_map/ppermute | solution.py:297
  4.9 9.8 %collective-permute-start.1 = (bf16[32,4224]{1,0:T(8,128)(2,1)S(1)}, bf16[32,4224]{1,0:T(8,128)(2,1)S(1)}, u32[]{:S(2)}, u32[]{:S(2)}) collective-permute-start(bf16[32,4224]{1,0:T(8,128)(2,1)S(1)} %get-tuple-element.95), channel_id=1, source_target_pairs={{0,16},{8,24},{16,0},{24,8},{1,17},{9,25},{17,1},{25,9},{2,18},{10... | collective-permute-start | bytes 811016 | tf_op jit(solution)/shard_map/ppermute | solution.py:297
  6.4 10.8 %collective-permute-start.6 = (bf16[32,4224]{1,0:T(8,128)(2,1)S(1)}, bf16[32,4224]{1,0:T(8,128)(2,1)S(1)}, u32[]{:S(2)}, u32[]{:S(2)}) collective-permute-start(bf16[32,4224]{1,0:T(8,128)(2,1)S(1)} %get-tuple-element.95), channel_id=1, source_target_pairs={{0,8},{8,0},{16,24},{24,16},{1,9},{9,1},{17,25},{25,17},{2,10},{10... | collective-permute-start | bytes 811016 | tf_op jit(solution)/shard_map/ppermute | solution.py:297
  6.9 11.7 %collective-permute-start.7 = (bf16[32,4224]{1,0:T(8,128)(2,1)S(1)}, bf16[32,4224]{1,0:T(8,128)(2,1)S(1)}, u32[]{:S(2)}, u32[]{:S(2)}) collective-permute-start(bf16[32,4224]{1,0:T(8,128)(2,1)S(1)} %get-tuple-element.94), channel_id=1, source_target_pairs={{0,16},{8,24},{16,0},{24,8},{1,17},{9,25},{17,1},{25,9},{2,18},{10... | collective-permute-start | bytes 811016 | tf_op jit(solution)/shard_map/ppermute | solution.py:297
  19.6 8.4 %collective-permute-start.2 = (bf16[32,4224]{1,0:T(8,128)(2,1)S(1)}, bf16[32,4224]{1,0:T(8,128)(2,1)S(1)}, u32[]{:S(2)}, u32[]{:S(2)}) collective-permute-start(bf16[32,4224]{1,0:T(8,128)(2,1)S(1)} %collective-permute-done.refs_0_), channel_id=1, source_target_pairs={{0,16},{8,24},{16,0},{24,8},{1,17},{9,25},{17,1},{25,9},{2,18},{10... | collective-permute-start | bytes 811016 | tf_op jit(solution)/shard_map/ppermute | solution.py:297
  21.1 8.1 %collective-permute-start.3 = (bf16[32,4224]{1,0:T(8,128)(2,1)S(1)}, bf16[32,4224]{1,0:T(8,128)(2,1)S(1)}, u32[]{:S(2)}, u32[]{:S(2)}) collective-permute-start(bf16[32,4224]{1,0:T(8,128)(2,1)S(1)} %collective-permute-done.1.refs_3_), channel_id=1, source_target_pairs={{0,8},{8,0},{16,24},{24,16},{1,9},{9,1},{17,25},{25,17},{2,10},{10... | collective-permute-start | bytes 811016 | tf_op jit(solution)/shard_map/ppermute | solution.py:297
  29.2 21.0 %collective-permute-start.17 = (bf16[1,64,2048]{2,1,0:T(8,128)(2,1)S(1)}, bf16[1,64,2048]{2,1,0:T(8,128)(2,1)S(1)}, u32[]{:S(2)}, u32[]{:S(2)}) collective-permute-start(bf16[1,64,2048]{2,1,0:T(8,128)(2,1)S(1)} %get-tuple-element.139), channel_id=1, source_target_pairs={{0,1},{1,0},{2,3},{3,2},{4,5},{5,4},{6,7},{7,6},{8,9},{9,8},{10,11... | collective-permute-start | bytes 786440 | tf_op jit(solution)/shard_map/ppermute | solution.py:297
  35.6 11.1 %collective-permute-start.13 = (bf16[64,2048]{1,0:T(8,128)(2,1)S(1)}, bf16[64,2048]{1,0:T(8,128)(2,1)S(1)}, u32[]{:S(2)}, u32[]{:S(2)}) collective-permute-start(bf16[64,2048]{1,0:T(8,128)(2,1)S(1)} %get-tuple-element.110), channel_id=1, source_target_pairs={{0,8},{8,0},{16,24},{24,16},{1,9},{9,1},{17,25},{25,17},{2,10},{10... | collective-permute-start | bytes 786440 | tf_op jit(solution)/shard_map/ppermute | solution.py:297
  36.2 10.6 %collective-permute-start.14 = (bf16[64,2048]{1,0:T(8,128)(2,1)S(1)}, bf16[64,2048]{1,0:T(8,128)(2,1)S(1)}, u32[]{:S(2)}, u32[]{:S(2)}) collective-permute-start(bf16[64,2048]{1,0:T(8,128)(2,1)S(1)} %get-tuple-element.111), channel_id=1, source_target_pairs={{0,16},{8,24},{16,0},{24,8},{1,17},{9,25},{17,1},{25,9},{2,18},{10... | collective-permute-start | bytes 786440 | tf_op jit(solution)/shard_map/ppermute | solution.py:297
  41.1 9.1 %collective-permute-start.16 = (bf16[64,2048]{1,0:T(8,128)(2,1)S(1)}, bf16[64,2048]{1,0:T(8,128)(2,1)S(1)}, u32[]{:S(2)}, u32[]{:S(2)}) collective-permute-start(bf16[64,2048]{1,0:T(8,128)(2,1)S(1)} %shard_map.201), channel_id=1, source_target_pairs={{0,24},{8,16},{16,8},{24,0},{1,25},{9,17},{17,9},{25,1},{2,26},{10... | collective-permute-start | bytes 786440 | tf_op jit(solution)/shard_map/ppermute | solution.py:297
  52.0 6.6 %collective-permute-start.19 = (bf16[16,2048]{1,0:T(8,128)(2,1)S(1)}, bf16[16,2048]{1,0:T(8,128)(2,1)S(1)}, u32[]{:S(2)}, u32[]{:S(2)}) collective-permute-start(bf16[16,2048]{1,0:T(8,128)(2,1)S(1)} %get-tuple-element.146), channel_id=1, source_target_pairs={{0,4},{1,5},{2,6},{3,7},{4,0},{5,1},{6,2},{7,3},{8,12},{9,13},{10,... | collective-permute-start | bytes 196616 | tf_op jit(solution)/shard_map/ppermute | solution.py:297
  54.6 6.4 %collective-permute-start.20 = (bf16[16,2048]{1,0:T(8,128)(2,1)S(1)}, bf16[16,2048]{1,0:T(8,128)(2,1)S(1)}, u32[]{:S(2)}, u32[]{:S(2)}) collective-permute-start(bf16[16,2048]{1,0:T(8,128)(2,1)S(1)} %get-tuple-element.147), channel_id=1, source_target_pairs={{0,6},{1,7},{2,4},{3,5},{4,2},{5,3},{6,0},{7,1},{8,14},{9,15},{10,... | collective-permute-start | bytes 196616 | tf_op jit(solution)/shard_map/ppermute | solution.py:297
  61.0 8.0 %collective-permute-start.21 = (bf16[16,2048]{1,0:T(8,128)(2,1)S(1)}, bf16[16,2048]{1,0:T(8,128)(2,1)S(1)}, u32[]{:S(2)}, u32[]{:S(2)}) collective-permute-start(bf16[16,2048]{1,0:T(8,128)(2,1)S(1)} %shard_map.202.refs_0_), channel_id=1, source_target_pairs={{0,2},{1,3},{2,0},{3,1},{4,6},{5,7},{6,4},{7,5},{8,10},{9,11},{10,... | collective-permute-start | bytes 196616 | tf_op jit(solution)/shard_map/ppermute | solution.py:297
  61.1 7.9 %collective-permute-start.22 = (bf16[16,2048]{1,0:T(8,128)(2,1)S(1)}, bf16[16,2048]{1,0:T(8,128)(2,1)S(1)}, u32[]{:S(2)}, u32[]{:S(2)}) collective-permute-start(bf16[16,2048]{1,0:T(8,128)(2,1)S(1)} %shard_map.202.refs_0_), channel_id=1, source_target_pairs={{0,4},{1,5},{2,6},{3,7},{4,0},{5,1},{6,2},{7,3},{8,12},{9,13},{10,... | collective-permute-start | bytes 196616 | tf_op jit(solution)/shard_map/ppermute | solution.py:297
  62.4 6.7 %collective-permute-start.23 = (bf16[16,2048]{1,0:T(8,128)(2,1)S(1)}, bf16[16,2048]{1,0:T(8,128)(2,1)S(1)}, u32[]{:S(2)}, u32[]{:S(2)}) collective-permute-start(bf16[16,2048]{1,0:T(8,128)(2,1)S(1)} %shard_map.202.refs_0_), channel_id=1, source_target_pairs={{0,6},{1,7},{2,4},{3,5},{4,2},{5,3},{6,0},{7,1},{8,14},{9,15},{10,... | collective-permute-start | bytes 196616 | tf_op jit(solution)/shard_map/ppermute | solution.py:297
  69.2 7.0 %collective-permute-start.24 = (bf16[64,512]{1,0:T(8,128)(2,1)S(1)}, bf16[64,512]{1,0:T(8,128)(2,1)S(1)}, u32[]{:S(2)}, u32[]{:S(2)}) collective-permute-start(bf16[64,512]{1,0:T(8,128)(2,1)S(1)} %get-tuple-element.156), channel_id=1, source_target_pairs={{0,8},{8,0},{16,24},{24,16},{1,9},{9,1},{17,25},{25,17},{2,10},{10... | collective-permute-start | bytes 196616 | tf_op jit(solution)/shard_map/ppermute | solution.py:297
  70.7 6.8 %collective-permute-start.25 = (bf16[64,512]{1,0:T(8,128)(2,1)S(1)}, bf16[64,512]{1,0:T(8,128)(2,1)S(1)}, u32[]{:S(2)}, u32[]{:S(2)}) collective-permute-start(bf16[64,512]{1,0:T(8,128)(2,1)S(1)} %get-tuple-element.157), channel_id=1, source_target_pairs={{0,16},{8,24},{16,0},{24,8},{1,17},{9,25},{17,1},{25,9},{2,18},{10... | collective-permute-start | bytes 196616 | tf_op jit(solution)/shard_map/ppermute | solution.py:297
  71.8 7.0 %collective-permute-start.26 = (bf16[64,512]{1,0:T(8,128)(2,1)S(1)}, bf16[64,512]{1,0:T(8,128)(2,1)S(1)}, u32[]{:S(2)}, u32[]{:S(2)}) collective-permute-start(bf16[64,512]{1,0:T(8,128)(2,1)S(1)} %get-tuple-element.158), channel_id=1, source_target_pairs={{0,24},{8,16},{16,8},{24,0},{1,25},{9,17},{17,9},{25,1},{2,26},{10... | collective-permute-start | bytes 196616 | tf_op jit(solution)/shard_map/ppermute | solution.py:297
  72.8 8.6 %collective-permute-start.30 = (bf16[128,256]{1,0:T(8,128)(2,1)S(1)}, bf16[128,256]{1,0:T(8,128)(2,1)S(1)}, u32[]{:S(2)}, u32[]{:S(2)}) collective-permute-start(bf16[128,256]{1,0:T(8,128)(2,1)S(1)} %copy-done.6), channel_id=1, source_target_pairs={{0,8},{8,0},{16,24},{24,16},{1,9},{9,1},{17,25},{25,17},{2,10},{10... | collective-permute-start | bytes 196616 | tf_op jit(solution)/shard_map/ppermute | solution.py:297
  74.2 12.0 %collective-permute-start.32 = (bf16[128,256]{1,0:T(8,128)(2,1)S(1)}, bf16[128,256]{1,0:T(8,128)(2,1)S(1)}, u32[]{:S(2)}, u32[]{:S(2)}) collective-permute-start(bf16[128,256]{1,0:T(8,128)(2,1)S(1)} %copy-done.6), channel_id=1, source_target_pairs={{0,16},{8,24},{16,0},{24,8},{1,17},{9,25},{17,1},{25,9},{2,18},{10... | collective-permute-start | bytes 196616 | tf_op jit(solution)/shard_map/ppermute | solution.py:297
  76.2 10.0 %collective-permute-start.35 = (bf16[144,128]{1,0:T(8,128)(2,1)S(1)}, bf16[144,128]{1,0:T(8,128)(2,1)S(1)}, u32[]{:S(2)}, u32[]{:S(2)}) collective-permute-start(bf16[144,128]{1,0:T(8,128)(2,1)S(1)} %get-tuple-element.170), channel_id=1, source_target_pairs={{8,0},{16,8},{24,16},{9,1},{17,9},{25,17},{10,2},{18,10},{26,18},{... | collective-permute-start | bytes 110600 | tf_op jit(solution)/shard_map/ppermute | solution.py:827
  77.5 9.2 %collective-permute-start.36 = (bf16[144,128]{1,0:T(8,128)(2,1)S(1)}, bf16[144,128]{1,0:T(8,128)(2,1)S(1)}, u32[]{:S(2)}, u32[]{:S(2)}) collective-permute-start(bf16[144,128]{1,0:T(8,128)(2,1)S(1)} %get-tuple-element.170), channel_id=1, source_target_pairs={{16,0},{24,8},{17,1},{25,9},{18,2},{26,10},{19,3},{27,11},{20,4},{... | collective-permute-start | bytes 110600 | tf_op jit(solution)/shard_map/ppermute | solution.py:827
  78.8 8.0 %collective-permute-start.37 = (bf16[144,128]{1,0:T(8,128)(2,1)S(1)}, bf16[144,128]{1,0:T(8,128)(2,1)S(1)}, u32[]{:S(2)}, u32[]{:S(2)}) collective-permute-start(bf16[144,128]{1,0:T(8,128)(2,1)S(1)} %get-tuple-element.170), channel_id=1, source_target_pairs={{24,0},{25,1},{26,2},{27,3},{28,4},{29,5},{30,6},{31,7}} | collective-permute-start | bytes 110600 | tf_op jit(solution)/shard_map/ppermute | solution.py:827
  81.4 7.3 %collective-permute-start.34 = (bf16[128,256]{1,0:T(8,128)(2,1)S(1)}, bf16[128,256]{1,0:T(8,128)(2,1)S(1)}, u32[]{:S(2)}, u32[]{:S(2)}) collective-permute-start(bf16[128,256]{1,0:T(8,128)(2,1)S(1)} %copy-done.6), channel_id=1, source_target_pairs={{0,24},{8,16},{16,8},{24,0},{1,25},{9,17},{17,9},{25,1},{2,26},{10... | collective-permute-start | bytes 196616 | tf_op jit(solution)/shard_map/ppermute | solution.py:297
  (22 other events, 121.8 us)
